TPU v7x, 256 devices: a whole 4x4x8 slice. The times are simulated.
256 devices in a mesh: sp: 32 (over z, x), tp: 4 (over y), dp: 2 (over core).
Axes of the slice: x: 4, y: 4, z: 8, core: 2. Of those that a mesh axis runs over, the one named last changes fastest.
Arguments:
- latent_in: bfloat16 [24576, 2048], P(('dp', 'sp', 'tp')), parts along dimension 0, may hold values from -6 to 6
- condition: bfloat16 [4096], P(('dp', 'sp')), parts along dimension 0, may hold values from -8 to 8
- context_latent: bfloat16 [1024, 256], P(('dp', 'sp')), parts along dimension 0, may hold values from -6 to 6
- context_rope: bfloat16 [1024, 64], P(('dp', 'sp')), parts along dimension 0, may hold values from -6 to 6
- shift_weight: bfloat16 [2048, 2048], P('sp', 'tp'), may hold values from -0.125 to 0.125
- scale_weight: bfloat16 [2048, 2048], P('sp', 'tp'), may hold values from -0.125 to 0.125
- gate_weight: bfloat16 [2048, 2048], P('sp', 'tp'), may hold values from -0.125 to 0.125
- norm_gain: float32 [2048], replicated, may hold values from 0.1 to 1.9
- down_query: bfloat16 [2048, 512], replicated, may hold values from -0.125 to 0.125
- down_latent: bfloat16 [2048, 256], replicated, may hold values from -0.125 to 0.125
- down_rope: bfloat16 [2048, 64], replicated, may hold values from -0.125 to 0.125
- query_gain: float32 [512], replicated, may hold values from 0.5 to 60
- latent_gain: float32 [256], replicated, may hold values from 0.1 to 1.9
- up_query: bfloat16 [512, 1536], P(None, 'tp'), may hold values from -0.25 to 0.25
- up_key: bfloat16 [256, 1024], P(None, 'tp'), may hold values from -0.375 to 0.375
- up_value: bfloat16 [256, 1024], P(None, 'tp'), may hold values from -0.375 to 0.375
- context_bias: float32 [8], P('tp'), may hold values from 1 to 2.5
- out_weight: bfloat16 [1024, 2048], replicated, may hold values from -3 to 3
Outputs:
- mixed_out: bfloat16 [24576, 2048], P(('dp', 'sp', 'tp')), parts along dimension 0
There are 2 independent parts, one for each index of `dp`. A program takes and returns all parts, laid end to end along the dimension named above; an argument that names none is the same for every part. Nothing has to cross between parts.
All inputs are finite; a program needn't handle non-finite values.
Results may differ from a plain program's by a relative error of at most 0.039.
The roundings to bfloat16 on the way count: a program that leaves them out, or rounds other values in their place, can miss the bound.
Values may be sent and summed in bfloat16 or wider, within the bound.
A program may use at most 128 MiB of HBM per device.

v0:
```python
import jax
import jax.numpy as jnp
from jax import lax
from jax.sharding import Mesh
from jax.sharding import PartitionSpec as P

QK_NOPE = 128
QK_ROPE = 64
V_HEAD = 128
GRID_W = 64
SP = ("sp_0", "sp_1")
DP_SP_TP = ("dp", "sp_0", "sp_1", "tp")
DP_SP = ("dp", "sp_0", "sp_1")


epsilon = 1e-06
rope_base = 10000.0
block_limit = 2048


def copy_for_each(value, axis):
    copies = jnp.broadcast_to(value, (lax.axis_size(axis), *value.shape))
    return lax.all_to_all(copies, axis, split_axis=0, concat_axis=0, tiled=True)


def taken_together(value, axis):
    everything = copy_for_each(value, axis)
    return jnp.sum(everything, axis=0)


def joined_along(pieces, dim):
    pieces = jnp.moveaxis(pieces, 0, dim)
    shape = pieces.shape
    return pieces.reshape(*shape[:dim], shape[dim] * shape[dim + 1], *shape[dim + 2 :])


def gather_directly(value, axis, dim):
    return joined_along(copy_for_each(value, axis), dim)


def gather_packed(arrays, axis, dims):
    ravelled = jnp.concatenate([a.reshape(-1) for a in arrays])
    lines, at, outs = (lax.all_gather(ravelled, axis), 0, [])
    for a, dim in zip(arrays, dims):
        pieces = lines[:, at : at + a.size].reshape(-1, *a.shape)
        outs.append(joined_along(pieces, dim))
        at += a.size
    return tuple(outs)


def whole_of(value, axes, dim):
    out = value
    for number in range(len(axes) - 1, -1, -1):
        out = lax.all_gather(out, axes[number], axis=dim, tiled=True)
    return out


def rms_scaled(values, gain_vec):
    mean_sq = jnp.mean(values * values, axis=-1, keepdims=True)
    return values * lax.rsqrt(mean_sq + epsilon) * gain_vec


def rope_tables(positions, rope_width):
    freq_count = rope_width // 4
    inverse = rope_base ** (-jnp.arange(freq_count, dtype=jnp.float32) / freq_count)
    grid_row = (positions // GRID_W).astype(jnp.float32)
    grid_col = (positions % GRID_W).astype(jnp.float32)
    row_angle = grid_row[:, None] * inverse
    col_angle = grid_col[:, None] * inverse
    angles = jnp.concatenate([row_angle, row_angle, col_angle, col_angle], axis=-1)
    return (jnp.cos(angles), jnp.sin(angles))


def rope_turn(values, cosine_table, sine_table):
    part_one, part_two, part_three, part_four = jnp.split(values, 4, axis=-1)
    turned = jnp.concatenate([-part_two, part_one, -part_four, part_three], axis=-1)
    return values * cosine_table + turned * sine_table


def attend(attn_state, query_nope, query_rope, keys_nope, values_in, keys_rope, bias_col):
    score_scale = (query_nope.shape[-1] + query_rope.shape[-1]) ** (-0.5)
    scores = jnp.einsum("thd,khd->htk", query_nope, keys_nope, preferred_element_type=jnp.float32)
    scores = scores + jnp.einsum(
        "thr,kr->htk", query_rope, keys_rope, preferred_element_type=jnp.float32
    )
    scores = scores * score_scale + bias_col
    run_max, run_total, run_acc = attn_state
    new_max = jnp.maximum(run_max, jnp.max(scores, axis=-1))
    shrink = jnp.exp(run_max - new_max)
    weights = jnp.exp(scores - new_max[:, :, None])
    new_total = run_total * shrink + jnp.sum(weights, axis=-1)
    new_acc = run_acc * shrink[:, :, None] + jnp.einsum(
        "htk,khd->htd", weights.astype(jnp.bfloat16), values_in, preferred_element_type=jnp.float32
    )
    return (new_max, new_total, new_acc)


def over_blocks(attn_state, arrays, handle):
    row_count = arrays[0].shape[0]
    block_rows = 1
    for candidate in range(min(row_count, block_limit), 0, -1):
        if row_count % candidate == 0:
            block_rows = candidate
            break
    block_count = row_count // block_rows
    if block_count == 1:
        return handle(attn_state, arrays)
    stacked = tuple(
        (array_in.reshape((block_count, block_rows) + array_in.shape[1:]) for array_in in arrays)
    )

    def one_turn(inner_state, pieces):
        return (handle(inner_state, pieces), None)

    return lax.scan(one_turn, attn_state, stacked)[0]


def on_device(
    latent_in,
    condition,
    context_latent,
    context_rope,
    shift_weight,
    scale_weight,
    gate_weight,
    norm_gain,
    down_query,
    down_latent,
    down_rope,
    query_gain,
    latent_gain,
    up_query,
    up_key,
    up_value,
    context_bias,
    out_weight,
):
    activated = jax.nn.silu(condition.astype(jnp.float32)).astype(jnp.bfloat16)
    partials = jnp.stack(
        [
            jnp.dot(activated, weight_in, preferred_element_type=jnp.float32)
            for weight_in in (shift_weight, scale_weight, gate_weight)
        ]
    )
    summed = taken_together(partials, SP)
    modulation = gather_directly(summed, "tp", 1)
    shift_vec = modulation[0]
    scale_vec = modulation[1]
    gate_vec = modulation[2]
    residual_in = latent_in.astype(jnp.float32)
    normed = (rms_scaled(residual_in, norm_gain) * (1.0 + scale_vec) + shift_vec).astype(
        jnp.bfloat16
    )
    query_low = rms_scaled(
        jnp.dot(normed, down_query, preferred_element_type=jnp.float32), query_gain
    ).astype(jnp.bfloat16)
    latent_low = rms_scaled(
        jnp.dot(normed, down_latent, preferred_element_type=jnp.float32), latent_gain
    ).astype(jnp.bfloat16)
    local_rows = latent_in.shape[0]
    first_row = (lax.axis_index(SP) * lax.axis_size("tp") + lax.axis_index("tp")) * local_rows
    own_positions = first_row + jnp.arange(local_rows, dtype=jnp.int32)
    own_cosine, own_sine = rope_tables(own_positions, QK_ROPE)
    rope_keys = rope_turn(
        jnp.dot(normed, down_rope, preferred_element_type=jnp.float32), own_cosine, own_sine
    ).astype(jnp.bfloat16)
    query_group, latent_group, rope_group = (
        lax.all_gather(query_low, "tp", axis=0, tiled=True),
        lax.all_gather(latent_low, "tp", axis=0, tiled=True),
        lax.all_gather(rope_keys, "tp", axis=0, tiled=True),
    )
    group_rows = query_group.shape[0]
    group_positions = lax.axis_index(SP) * group_rows + jnp.arange(group_rows, dtype=jnp.int32)
    group_cosine, group_sine = rope_tables(group_positions, QK_ROPE)
    head_count = up_key.shape[1] // QK_NOPE
    queries = jnp.dot(query_group, up_query, preferred_element_type=jnp.float32).reshape(
        group_rows, head_count, QK_NOPE + QK_ROPE
    )
    query_nope = queries[:, :, :QK_NOPE].astype(jnp.bfloat16)
    query_rope = rope_turn(
        queries[:, :, QK_NOPE:], group_cosine[:, None, :], group_sine[:, None, :]
    ).astype(jnp.bfloat16)
    context_all, context_keys_rope = gather_packed((context_latent, context_rope), SP, (0, 0))
    context_count = context_all.shape[0]
    context_nope = (
        jnp.dot(context_all, up_key, preferred_element_type=jnp.float32)
        .astype(jnp.bfloat16)
        .reshape(context_count, head_count, QK_NOPE)
    )
    context_values = (
        jnp.dot(context_all, up_value, preferred_element_type=jnp.float32)
        .astype(jnp.bfloat16)
        .reshape(context_count, head_count, V_HEAD)
    )
    start_state = (
        jnp.full((head_count, group_rows), -jnp.inf, jnp.float32),
        jnp.zeros((head_count, group_rows), jnp.float32),
        jnp.zeros((head_count, group_rows, V_HEAD), jnp.float32),
    )
    bias_col = context_bias[:, None, None]

    def context_step(inner_state, pieces):
        return attend(
            inner_state, query_nope, query_rope, pieces[0], pieces[1], pieces[2], bias_col
        )

    attn_state = over_blocks(
        start_state, (context_nope, context_values, context_keys_rope), context_step
    )

    def latent_step(inner_state, pieces):
        piece_rows = pieces[0].shape[0]
        piece_nope = jnp.dot(pieces[0], up_key, preferred_element_type=jnp.float32).astype(
            jnp.bfloat16
        )
        piece_values = jnp.dot(pieces[0], up_value, preferred_element_type=jnp.float32).astype(
            jnp.bfloat16
        )
        return attend(
            inner_state,
            query_nope,
            query_rope,
            piece_nope.reshape(piece_rows, head_count, QK_NOPE),
            piece_values.reshape(piece_rows, head_count, V_HEAD),
            pieces[1],
            0.0,
        )

    attn_state = over_blocks(
        attn_state, (whole_of(latent_group, SP, 0), whole_of(rope_group, SP, 0)), latent_step
    )
    attended = (attn_state[2] / attn_state[1][:, :, None]).astype(jnp.bfloat16)
    attended = attended.transpose(1, 0, 2).reshape(group_rows, head_count * V_HEAD)
    token_major = lax.all_to_all(attended, "tp", split_axis=0, concat_axis=1, tiled=True)
    mixed = jnp.dot(token_major, out_weight, preferred_element_type=jnp.float32)
    return (residual_in + gate_vec * mixed).astype(jnp.bfloat16)


def solution(mesh):
    split = Mesh(
        mesh.devices.reshape(8, 4, mesh.shape["tp"], mesh.shape["dp"]), ("sp_0", "sp_1", "tp", "dp")
    )
    placed = (
        P(DP_SP_TP, None),
        P(DP_SP),
        P(DP_SP, None),
        P(DP_SP, None),
        P(SP, "tp"),
        P(SP, "tp"),
        P(SP, "tp"),
        P(),
        P(),
        P(),
        P(),
        P(),
        P(),
        P(None, "tp"),
        P(None, "tp"),
        P(None, "tp"),
        P("tp"),
        P(),
    )
    return jax.shard_map(
        on_device, mesh=split, in_specs=placed, out_specs=P(DP_SP_TP, None), check_vma=False
    )
```

profile of v0, /device:TPU:2, one launch (start us, length us, event | category | flops | bytes accessed | tf_op | source)
XLA Modules:
  0.0 259.0 jit_solution(644855373006854775)
XLA Ops:
  6.5 1.1 fusion.47
  7.7 1.0 fusion.49
  8.7 1.0 fusion.51
  10.4 11.6 %all-to-all-start = ((f32[32,3,512]{2,1,0:T(4,128)}), f32[32,3,512]{2,1,0:T(4,128)S(1)}, u32[]{:S(2)}, u32[]{:S(2)}) async-start(f32[32,3,512]{2,1,0:T(4,128)} %broadcast_in_dim.8), calls=%async_computation | async-start | bytes 524288 | tf_op jit(solution)/shard_map/all_to_all | solution.py:23
  22.1 1.2 fusion.25
  23.3 9.9 %all-to-all-done = f32[32,3,512]{2,1,0:T(4,128)S(1)} async-done(((f32[32,3,512]{2,1,0:T(4,128)}), f32[32,3,512]{2,1,0:T(4,128)S(1)}, u32[]{:S(2)}, u32[]{:S(2)}) %all-to-all-start) | async-done | bytes 196640 | tf_op jit(solution)/shard_map/all_to_all | solution.py:23
  33.9 4.5 %all-to-all-start.1 = ((f32[4,3,512]{2,1,0:T(4,128)}), f32[4,3,512]{2,1,0:T(4,128)S(1)}, u32[]{:S(2)}, u32[]{:S(2)}) async-start(f32[4,3,512]{2,1,0:T(4,128)} %broadcast_in_dim.9), calls=%async_computation.1 | async-start | bytes 65536 | tf_op jit(solution)/shard_map/all_to_all | solution.py:23
  38.4 5.4 %all-to-all-done.1 = f32[4,3,512]{2,1,0:T(4,128)S(1)} async-done(((f32[4,3,512]{2,1,0:T(4,128)}), f32[4,3,512]{2,1,0:T(4,128)S(1)}, u32[]{:S(2)}, u32[]{:S(2)}) %all-to-all-start.1) | async-done | bytes 24608 | tf_op jit(solution)/shard_map/all_to_all | solution.py:23
  43.9 1.4 fusion.58
  45.4 11.9 %all-gather.1 = bf16[4,96,64]{1,2,0:T(8,128)(2,1)S(1)} all-gather(bf16[1,96,64]{1,2,0:T(8,128)(2,1)S(1)} %fusion.40), channel_id=1, replica_groups=mesh['sp_0'=8,'sp_1'=4,'tp'=4,'dp'=2] {'tp'}, dimensions={0}, use_global_device_ids=true | all-gather | bytes 61440 | tf_op jit(solution)/shard_map/all_gather | solution.py:170
  57.5 13.0 %all_gather.34 = bf16[1536,64]{0,1:T(8,128)(2,1)} all-gather(bf16[384,64]{0,1:T(8,128)(2,1)S(1)} %reshape.263), channel_id=1, replica_groups=mesh['sp_0'=8,'sp_1'=4,'tp'=4,'dp'=2] {'sp_1'}, dimensions={0}, use_global_device_ids=true | all-gather | bytes 245760 | tf_op jit(solution)/shard_map/all_gather | solution.py:54
  70.6 1.7 multiply_reduce_fusion.1
  72.4 12.1 %all_gather.30 = bf16[384,256]{1,0:T(8,128)(2,1)S(1)} all-gather(bf16[96,256]{1,0:T(8,128)(2,1)S(1)} %multiply_convert_fusion.1), channel_id=1, replica_groups=mesh['sp_0'=8,'sp_1'=4,'tp'=4,'dp'=2] {'tp'}, dimensions={0}, use_global_device_ids=true | all-gather | bytes 245760 | tf_op jit(solution)/shard_map/all_gather | solution.py:169
  84.5 14.1 %all_gather.31 = bf16[1536,256]{1,0:T(8,128)(2,1)} all-gather(bf16[384,256]{1,0:T(8,128)(2,1)S(1)} %all_gather.30), channel_id=1, replica_groups=mesh['sp_0'=8,'sp_1'=4,'tp'=4,'dp'=2] {'sp_1'}, dimensions={0}, use_global_device_ids=true | all-gather | bytes 983040 | tf_op jit(solution)/shard_map/all_gather | solution.py:54
  98.8 54.1 %all-gather = bf16[163840]{0:T(1024)(128)(2,1)} all-gather(bf16[5120]{0:T(1024)(128)(2,1)S(1)} %pad_maximum_fusion.2), channel_id=2, replica_groups=mesh['sp_0'=8,'sp_1'=4,'tp'=4,'dp'=2] {'sp_0','sp_1'}, dimensions={0}, use_global_device_ids=true | all-gather | bytes 337920 | tf_op jit(solution)/shard_map/all_gather | solution.py:43
  152.9 1.1 reshape.261
  154.8 1.1 reshape_reshape.6
  156.7 0.9 fusion.37
  157.6 1.0 convolution_convert_fusion.3
  159.6 12.7 %all_gather.27 = bf16[384,512]{1,0:T(8,128)(2,1)S(1)} all-gather(bf16[96,512]{1,0:T(8,128)(2,1)S(1)} %multiply_convert_fusion), channel_id=1, replica_groups=mesh['sp_0'=8,'sp_1'=4,'tp'=4,'dp'=2] {'tp'}, dimensions={0}, use_global_device_ids=true | all-gather | bytes 491520 | tf_op jit(solution)/shard_map/all_gather | solution.py:168
  173.5 1.1 copy.85
  174.6 1.0 fusion.33
  175.6 1.4 fusion.67
  176.9 1.4 fusion.66
  179.3 2.8 %copy.103 = bf16[8,6,8,2048]{3,2,0,1:T(8,128)(2,1)} copy(bf16[8,6,8,2048]{3,2,1,0:T(8,128)(2,1)} %bitcast.116) | data formatting | bytes 3145728 | tf_op jit(solution)/shard_map/reshape | solution.py:109
  182.1 55.6 %while.14 = (s32[]{:T(128)}, f32[2,384]{1,0:T(2,128)S(1)}, f32[2,384]{1,0:T(2,128)S(1)}, f32[2,384,128]{2,1,0:T(8,128)S(1)}, bf16[6,2048,256]{2,1,0:T(8,128)(2,1...) while((s32[]{:T(128)}, f32[2,384]{1,0:T(2,128)S(1)}, ...), condition=%wide.region_9.10_spmd, body=%wide.region_6.9_spmd.sunk | while | flops 1555760640 | bytes 39405164 | solution.py:115
  182.1 1.7 convolution_convert_fusion.6
  183.9 2.0 fusion.117
  185.8 1.3 fusion.118
  187.2 0.8 fusion.119
  188.0 1.7 convolution_convert_fusion.7
  189.8 1.6 fusion.120
  191.4 1.7 convolution_convert_fusion.6
  193.1 2.0 fusion.117
  195.1 1.3 fusion.118
  196.5 0.8 fusion.119
  197.3 1.7 convolution_convert_fusion.7
  199.0 1.6 fusion.120
  200.7 1.7 convolution_convert_fusion.6
  202.4 2.0 fusion.117
  204.4 1.3 fusion.118
  205.7 0.8 fusion.119
  206.6 1.7 convolution_convert_fusion.7
  208.3 1.6 fusion.120
  210.0 1.7 convolution_convert_fusion.6
  211.7 2.0 fusion.117
  213.6 1.3 fusion.118
  215.0 0.8 fusion.119
  215.9 1.7 convolution_convert_fusion.7
  217.6 1.6 fusion.120
  219.2 1.7 convolution_convert_fusion.6
  220.9 2.0 fusion.117
  222.9 1.3 fusion.118
  224.3 0.8 fusion.119
  225.1 1.7 convolution_convert_fusion.7
  226.8 1.6 fusion.120
  228.5 1.7 convolution_convert_fusion.6
  230.2 2.0 fusion.117
  232.2 1.3 fusion.118
  233.5 0.8 fusion.119
  234.4 1.7 convolution_convert_fusion.7
  236.1 1.6 fusion.120
  238.3 10.1 %all_to_all.29 = bf16[4,96,256]{2,1,0:T(8,128)(2,1)S(1)} all-to-all(bf16[4,96,256]{2,1,0:T(8,128)(2,1)S(1)} %all_to_all.22), channel_id=1, replica_groups=mesh['sp_0'=8,'sp_1'=4,'tp'=4,'dp'=2] {'tp'}, dimensions={0} | all-to-all | bytes 393216 | tf_op jit(solution)/shard_map/all_to_all | solution.py:234
  248.4 3.8 %fusion.20 = bf16[96,2048]{1,0:T(8,128)(2,1)} fusion(bf16[96,1024]{1,0:T(8,128)(2,1)S(1)} %bitcast.119, bf16[1024,2048]{1,0:T(8,128)(2,1)} %param.37, bf16[96,2048]{1,0:T(8,128)(2,1)S(1)} %copy-done.4, f32[2048]{0:T(1024)S(1)} %bitcast.122), kind=kOutput, calls=%fused_computation.24 | convolution fusion | flops 403439616 | bytes 5185536 | tf_op jit(solution)/shard_map/dot_general | solution.py:235
  (85 shorter events, 7.5 us)
Async XLA Ops:
  6.5 152.4 %copy-start = (bf16[2048,512]{1,0:T(8,128)(2,1)S(1)}, bf16[2048,512]{1,0:T(8,128)(2,1)}, u32[]{:S(2)}) copy-start(bf16[2048,512]{1,0:T(8,128)(2,1)} %param.28) | copy-start | bytes 6291460
  6.5 64.0 %copy-start.3 = (bf16[96,2048]{1,0:T(8,128)(2,1)S(1)}, bf16[96,2048]{1,0:T(8,128)(2,1)}, u32[]{:S(2)}) copy-start(bf16[96,2048]{1,0:T(8,128)(2,1)} %param.20) | copy-start | bytes 1179652
  6.5 64.0 %copy-start.11 = (f32[2048]{0:T(1024)S(1)}, f32[2048]{0:T(1024)}, u32[]{:S(2)}) copy-start(f32[2048]{0:T(1024)} %param.27) | copy-start | bytes 24580
  10.4 22.8 %all-to-all-start = ((f32[32,3,512]{2,1,0:T(4,128)}), f32[32,3,512]{2,1,0:T(4,128)S(1)}, u32[]{:S(2)}, u32[]{:S(2)}) async-start(f32[32,3,512]{2,1,0:T(4,128)} %broadcast_in_dim.8), calls=%async_computation | async-start | bytes 524288 | tf_op jit(solution)/shard_map/all_to_all | solution.py:23
  33.9 9.9 %all-to-all-start.1 = ((f32[4,3,512]{2,1,0:T(4,128)}), f32[4,3,512]{2,1,0:T(4,128)S(1)}, u32[]{:S(2)}, u32[]{:S(2)}) async-start(f32[4,3,512]{2,1,0:T(4,128)} %broadcast_in_dim.9), calls=%async_computation.1 | async-start | bytes 65536 | tf_op jit(solution)/shard_map/all_to_all | solution.py:23
  38.4 140.9 %all-gather.7.cloned.1.call-start = ((), (), s32[]{:S(2)}) async-start(), calls=%async_computation.4 | async-start | bytes 1769472 | tf_op jit(solution)/shard_map/all_gather | solution.py:54
  43.9 28.4 %copy-start.9 = (f32[256]{0:T(256)S(1)}, f32[256]{0:T(256)}, u32[]{:S(2)}) copy-start(f32[256]{0:T(256)} %param.32) | copy-start | bytes 3076
  70.5 28.2 %copy-start.6 = (bf16[16,256]{1,0:T(8,128)(2,1)S(1)}, bf16[16,256]{1,0:T(8,128)(2,1)}, u32[]{:S(2)}) copy-start(bf16[16,256]{1,0:T(8,128)(2,1)} %param.22) | copy-start | bytes 24580
  70.5 28.2 %copy-start.7 = (bf16[16,64]{1,0:T(8,128)(2,1)S(1)}, bf16[16,64]{1,0:T(8,128)(2,1)}, u32[]{:S(2)}) copy-start(bf16[16,64]{1,0:T(8,128)(2,1)} %param.23) | copy-start | bytes 6148
  70.5 111.7 %all-gather.5.cloned.1.call-start = ((), (), s32[]{:S(2)}) async-start(), calls=%async_computation.3 | async-start | bytes 7077888 | tf_op jit(solution)/shard_map/all_gather | solution.py:54
  84.5 73.1 %copy-start.1 = (bf16[256,256]{1,0:T(8,128)(2,1)S(1)}, bf16[256,256]{1,0:T(8,128)(2,1)}, u32[]{:S(2)}) copy-start(bf16[256,256]{1,0:T(8,128)(2,1)} %param.34) | copy-start | bytes 393220
  98.6 60.0 %copy-start.2 = (bf16[256,256]{1,0:T(8,128)(2,1)S(1)}, bf16[256,256]{1,0:T(8,128)(2,1)}, u32[]{:S(2)}) copy-start(bf16[256,256]{1,0:T(8,128)(2,1)} %param.35) | copy-start | bytes 393220
  157.6 1.9 copy-start.8
  158.6 13.7 %copy-start.5 = (bf16[512,384]{1,0:T(8,128)(2,1)S(1)}, bf16[512,384]{1,0:T(8,128)(2,1)}, u32[]{:S(2)}) copy-start(bf16[512,384]{1,0:T(8,128)(2,1)} %param.33) | copy-start | bytes 1179652
  172.8 4.2 %copy-start.10 = (f32[2]{0:T(128)S(1)}, f32[2]{0:T(128)}, u32[]{:S(2)}) copy-start(f32[2]{0:T(128)} %param.36) | copy-start | bytes 28
  237.8 10.6 %copy-start.4 = (bf16[96,2048]{1,0:T(8,128)(2,1)S(1)}, bf16[96,2048]{1,0:T(8,128)(2,1)}, u32[]{:S(2)}) copy-start(bf16[96,2048]{1,0:T(8,128)(2,1)} %param.20) | copy-start | bytes 1179652
Sparse Core Ops, SparseCore 0:
  70.6 34.6 all-gather.6
  107.1 74.6 all-gather.4
where the time goes:
time: 260 us; the launch traced here: 259 us
  blocking collectives  128 us (49%)
  matrix products  65.6 us (25%)
  starting transfers between devices  16.1 us (6%)
  waiting for transfers between devices  15.4 us (6%)
  between operations  13.7 us (5%)
  local copies, waits for them, and re-layouts  10.4 us (4%)
  other arithmetic  9.4 us (4%)
    all_gather x1, blocking collectives, gather_packed(): lines, at, outs = (lax.all_gather(ravelled, axis), 0, [])  54.1 us
    all_gather x2, blocking collectives, whole_of(): out = lax.all_gather(out, axes[number], axis=dim, tiled=True)  27.1 us
    all_to_all x2, starting transfers between devices, copy_for_each(): return lax.all_to_all(copies, axis, split_axis=0, concat_axis=0, tiled=True)  16.1 us
    all_to_all x2, waiting for transfers between devices, copy_for_each(): return lax.all_to_all(copies, axis, split_axis=0, concat_axis=0, tiled=True)  15.4 us
    dot_general x7, matrix products, attend(): jnp.einsum('thr,kr->htk', query_rope, keys_rope, preferred_element_type=j...  13.2 us
    all_gather x1, blocking collectives, on_device(): lax.all_gather(query_low, 'tp', axis=0, tiled=True)  12.7 us
    all_gather x1, blocking collectives, on_device(): lax.all_gather(latent_low, 'tp', axis=0, tiled=True)  12.1 us
    all_gather x1, blocking collectives, on_device(): lax.all_gather(rope_keys, 'tp', axis=0, tiled=True)  11.9 us
  transfers between devices with their start and end apart: 4, of which 2 were waited for; matrix products, arithmetic and copies ran while one was open for 8% of the time, Pallas kernels for 0%

commit v1 on v0

v1 whole, which is shorter than its diff:
```python
import functools
import math

import jax
import jax.numpy as jnp
from jax import lax
from jax.experimental import pallas as pl
from jax.experimental.pallas import tpu as pltpu
from jax.sharding import Mesh
from jax.sharding import PartitionSpec as P

ROWS = 96
D = 2048
NZ, NX, NY = 8, 4, 4
GRID_W = 64
CTXK = 128
EPS = 1e-06
QN = NY * ROWS
BUNDLE = NX * ROWS
LOG2E = math.log2(math.e)
SCALE2 = LOG2E / math.sqrt(192.0)
MESH = pl.DeviceIdType.MESH
F32 = jnp.float32
BF16 = jnp.bfloat16
NEG = float("-inf")


def dot(a, b):
    return jnp.dot(a, b, preferred_element_type=F32)


def dot_nt(a, b):
    return lax.dot_general(a, b, (((1,), (1,)), ((), ())), preferred_element_type=F32)


def remote(src, dst, send_sem, recv_sem, **where):
    return pltpu.make_async_remote_copy(
        src_ref=src, dst_ref=dst, send_sem=send_sem, recv_sem=recv_sem,
        device_id=where, device_id_type=MESH,
    )


def greet(peers):
    barrier = pltpu.get_barrier_semaphore()
    for where in peers:
        pl.semaphore_signal(barrier, inc=1, device_id=where, device_id_type=MESH)
    pl.semaphore_wait(barrier, len(peers))


def prepare_kernel(
    cond, sw, cw, gw, bias, lat, gain, qg, lg, cosr, sinr, ctxl, ctxr,
    dq_h, dl_h, dr_h, uq_h, uk_h, uv_h,
    qlow_o, kblk_o, gate_o, bias_o, ctx_o, uq, uk, uv,
    dq, dl, dr, mod_x, mod_z, mod_y, cblk, cx,
    down_sem, own_sem, xs, xr, zs, zr, ys, yr, cxs, cxr, czs, czr, ws, wr, fs, fr,
):
    z, x, y, c = (lax.axis_index(n) for n in ("z", "x", "y", "c"))
    downs = [
        pltpu.make_async_copy(h, v, down_sem.at[i])
        for i, (h, v) in enumerate(((dq_h, dq), (dl_h, dl), (dr_h, dr)))
    ]
    owns = [
        pltpu.make_async_copy(h, v.at[y], own_sem.at[i])
        for i, (h, v) in enumerate(((uq_h, uq), (uk_h, uk), (uv_h, uv)))
    ]
    for copy in owns + downs:
        copy.start()
    xp = [lax.rem(x + d, NX) for d in range(NX)]
    yp = [lax.rem(y + d, NY) for d in range(NY)]
    zp = [lax.rem(z + d, NZ) for d in range(NZ)]
    greet(
        [{"x": xp[d]} for d in range(1, NX)]
        + [{"y": yp[d]} for d in range(1, NY)]
        + [{"z": zp[d]} for d in range(1, NZ)]
        + [{"c": 1 - c}]
    )
    v = cond[...].astype(F32)
    activated = (v / (1.0 + jnp.exp(-v))).astype(BF16)
    part = jnp.concatenate([dot(activated, w[...]) for w in (sw, cw, gw)], axis=0)
    mod_x[x] = part
    xcopies = [
        remote(mod_x.at[x], mod_x.at[x], xs.at[d], xr.at[d], x=xp[d]) for d in range(1, NX)
    ]
    for copy in xcopies:
        copy.start()
    cblk[...] = jnp.concatenate(
        [ctxl[...], ctxr[...], jnp.zeros((16, 64), BF16)], axis=1
    )
    cx[x] = cblk[...]
    ccopies = [remote(cblk, cx.at[x], cxs.at[d], cxr.at[d], x=xp[d]) for d in range(1, NX)]
    for copy in ccopies:
        copy.start()
    for copy in owns:
        copy.wait()

    def half(ref, slot, core):
        rows = ref.shape[1] // 2
        return ref.at[slot, pl.ds(pl.multiple_of(core * rows, rows), rows)]

    wcopies = [
        [
            remote(half(w, y, c), half(w, y, c), ws.at[d, i], wr.at[d, i], y=yp[d])
            for i, w in enumerate((uq, uk, uv))
        ]
        for d in range(1, NY)
    ]
    for copy in xcopies:
        copy.wait_recv()
    mod_z[z] = mod_x[0] + mod_x[1] + mod_x[2] + mod_x[3]
    zcopies = [
        remote(mod_z.at[z], mod_z.at[z], zs.at[d], zr.at[d], z=zp[d]) for d in range(1, NZ)
    ]
    for copy in zcopies:
        copy.start()
    for d in (1, 3):
        wcopies[d - 1][0].start()
    lat32 = lat[...].astype(F32)
    inv = lax.rsqrt(jnp.mean(lat32 * lat32, axis=-1, keepdims=True) + EPS)
    for copy in ccopies:
        copy.wait_recv()
    mine = z // 2 == y
    first = (z % 2) * 64
    zc = [
        remote(
            cx, ctx_o.at[pl.ds(pl.multiple_of((z % 2) * NX, NX), NX)], czs.at[d],
            czr.at[z % 2], z=zp[d],
        )
        for d in range(1, NZ)
    ]

    @pl.when(mine)
    def _():
        ctx_o[pl.ds((z % 2) * NX, NX)] = cx[...]
        for copy in zc:
            copy.start()

    for copy in zcopies:
        copy.wait_recv()
    total = mod_z[0]
    for k in range(1, NZ):
        total = total + mod_z[k]
    lane = lax.broadcasted_iota(jnp.int32, (1, 512), 1)
    bias_row = jnp.where(lane == 0, bias[0], jnp.where(lane == 1, bias[1], 0.0))
    mod_y[y] = jnp.concatenate([total, bias_row], axis=0)
    ycopies = [
        remote(mod_y.at[y], mod_y.at[y], ys.at[d], yr.at[d], y=yp[d]) for d in range(1, NY)
    ]
    for copy in ycopies:
        copy.start()
    for d in (1, 3):
        for i in (1, 2):
            wcopies[d - 1][i].start()
    for copy in wcopies[1]:
        copy.start()
    for copy in ycopies:
        copy.wait_recv()
    shift = jnp.concatenate([mod_y[k, 0:1] for k in range(NY)], axis=1)
    scale = jnp.concatenate([mod_y[k, 1:2] for k in range(NY)], axis=1)
    gate_o[...] = jnp.concatenate([mod_y[k, 2:3] for k in range(NY)], axis=1)
    bias_o[...] = jnp.concatenate([mod_y[k, 3:4, 0:128] for k in range(NY)], axis=0)
    normed = (lat32 * inv * gain[...] * (1.0 + scale) + shift).astype(BF16)
    for copy in downs:
        copy.wait()

    def rms(a, g):
        return a * lax.rsqrt(jnp.mean(a * a, axis=-1, keepdims=True) + EPS) * g

    qlow_o[...] = rms(dot(normed, dq[...]), qg[...]).astype(BF16)
    low = rms(dot(normed, dl[...]), lg[...]).astype(BF16)
    u = dot(normed, dr[...])
    turned = jnp.concatenate([-u[:, 16:32], u[:, 0:16], -u[:, 48:64], u[:, 32:48]], axis=1)
    rope = (u * cosr[...] + turned * sinr[...]).astype(BF16)
    kblk_o[...] = jnp.concatenate([low, rope, jnp.zeros((ROWS, 64), BF16)], axis=1)
    forwards = []
    for d in (1, 3, 2):
        slot = lax.rem(y - d + NY, NY)
        for i, w in enumerate((uq, uk, uv)):
            wcopies[d - 1][i].wait_recv()
            copy = remote(half(w, slot, c), half(w, slot, c), fs.at[d, i], fr.at[d, i], c=1 - c)
            copy.start()
            forwards.append(copy)
    for copy in forwards:
        copy.wait()

    for k in range(2):
        @pl.when(z != 2 * y + k)
        def _():
            remote(cx, ctx_o.at[pl.ds(k * NX, NX)], czs.at[0], czr.at[k], z=zp[1]).wait_recv()

    @pl.when(mine)
    def _():
        for copy in zc:
            copy.wait_send()

    for copy in xcopies + ccopies + zcopies + ycopies + sum(wcopies, []):
        copy.wait_send()


def attend_kernel(
    qlow, kblk, uq, uk, uv, ctx, bias, cos_t, sin_t,
    out,
    qa, zk, wq_t, wv_t, q_t, m_s, l_s, acc, ob, rb, lse, sb, rsb,
    qs, qr, xs, xr, rs, rr, ls, lr, os, orr, ss, sr,
):
    z, x, y = (lax.axis_index(n) for n in ("z", "x", "y"))
    xp = [lax.rem(x + d, NX) for d in range(NX)]
    yp = [lax.rem(y + d, NY) for d in range(NY)]
    right, left = lax.rem(z + 1, NZ), lax.rem(z + NZ - 1, NZ)
    greet(
        [{"x": xp[d]} for d in range(1, NX)]
        + [{"y": yp[d]} for d in range(1, NY)]
        + [{"z": right}, {"z": left}]
    )
    kcopies = [
        remote(kblk, zk.at[z, x], xs.at[d], xr.at[d], x=xp[d]) for d in range(1, NX)
    ]
    qcopies = [remote(qlow, qa.at[y], qs.at[d], qr.at[d], y=yp[d]) for d in range(1, NY)]
    for copy in kcopies + qcopies:
        copy.start()
    qa[y] = qlow[...]
    zk[z, x] = kblk[...]
    for k in range(NY):
        wq_t[k] = uq[k].T
        wv_t[k] = uv[k].T
    m_s[...] = jnp.full(m_s.shape, NEG, F32)
    l_s[...] = jnp.zeros(l_s.shape, F32)
    acc[...] = jnp.zeros(acc.shape, F32)

    for copy in kcopies:
        copy.wait_recv()

    def slot_of(offset):
        return lax.rem(z + offset + NZ, NZ)

    def send_right(s):
        k = slot_of(1 - s)
        return remote(zk.at[k], zk.at[k], rs.at[s], rr.at[s], z=right)

    def send_left(s):
        k = slot_of(s - 1)
        return remote(zk.at[k], zk.at[k], ls.at[s], lr.at[s], z=left)

    last_right = remote(
        zk.at[slot_of(-3), pl.ds(0, 2)], zk.at[slot_of(-3), pl.ds(0, 2)],
        rs.at[4], rr.at[4], z=right,
    )
    last_left = remote(
        zk.at[slot_of(3), pl.ds(2, 2)], zk.at[slot_of(3), pl.ds(2, 2)],
        ls.at[4], lr.at[4], z=left,
    )
    send_right(1).start()
    send_left(1).start()

    for copy in qcopies:
        copy.wait_recv()

    @pl.loop(0, NY)
    def _(k):
        qt = dot_nt(wq_t[k], qa[...].reshape(QN, 512))
        for h in range(2):
            b = 192 * h
            u = qt[b + 128 : b + 192]
            turned = jnp.concatenate([-u[16:32], u[0:16], -u[48:64], u[32:48]], axis=0)
            rope = u * cos_t[...] + turned * sin_t[...]
            q_t[2 * k + h] = jnp.concatenate(
                [qt[b : b + 128], rope, jnp.zeros((64, QN), F32)], axis=0
            ).astype(BF16)

    def process(load, biased):
        @pl.loop(0, NY)
        def _(k):
            keys = load()
            low, rope = keys[:, :256], keys[:, 256:]
            nope = dot(low, uk[k]).astype(BF16)
            val_t = dot_nt(wv_t[k], low).astype(BF16)
            for h in range(2):
                head = 2 * k + h
                key = jnp.concatenate([nope[:, 128 * h : 128 * h + 128], rope], axis=1)
                s = dot(key, q_t[head]) * SCALE2
                if biased:
                    s = s + bias[pl.ds(k, 1), h : h + 1] * LOG2E
                m_old = m_s[head]
                m_new = jnp.maximum(m_old, jnp.max(s, axis=0, keepdims=True))
                p = jnp.exp2(s - m_new)
                shrink = jnp.exp2(m_old - m_new)
                l_s[head] = l_s[head] * shrink + jnp.sum(p, axis=0, keepdims=True)
                acc[head] = acc[head] * shrink + dot(
                    val_t[128 * h : 128 * h + 128], p.astype(BF16)
                )
                m_s[head] = m_new

    process(lambda: ctx[...].reshape(CTXK, 384), True)
    process(lambda: zk[z].reshape(BUNDLE, 384), False)

    @pl.loop(1, 4)
    def _(s):
        send_right(s).wait_recv()
        send_left(s).wait_recv()

        @pl.when(s < 3)
        def _():
            send_right(s + 1).start()
            send_left(s + 1).start()

        @pl.when(s == 3)
        def _():
            last_right.start()
            last_left.start()

        process(
            lambda: jnp.concatenate(
                [zk[slot_of(-s)].reshape(BUNDLE, 384), zk[slot_of(s)].reshape(BUNDLE, 384)],
                axis=0,
            ),
            False,
        )

    last_right.wait_recv()
    last_left.wait_recv()
    process(lambda: zk[slot_of(4)].reshape(BUNDLE, 384), False)

    for k in range(NY):
        both = []
        for h in range(2):
            head = 2 * k + h
            total = l_s[head]
            both.append((acc[head] / total).T)
            lse[head : head + 1] = m_s[head] + jnp.log2(total)
        ob[k] = jnp.concatenate(both, axis=1).astype(BF16).reshape(NY, ROWS, 256)
        for d in range(1, NY):
            remote(ob.at[k, yp[d]], rb.at[d, k], os.at[d, k], orr.at[d, k], y=yp[d]).start()
    sb[...] = jnp.concatenate([lse[...], jnp.zeros((120, QN), F32)], axis=0).T.reshape(
        NY, ROWS, 128
    )
    for d in range(1, NY):
        remote(sb.at[yp[d]], rsb.at[d], ss.at[d], sr.at[d], y=yp[d]).start()
    for d in range(1, NY):
        remote(sb.at[yp[d]], rsb.at[d], ss.at[d], sr.at[d], y=yp[d]).wait_recv()
    stats = [sb[y]] + [rsb[d] for d in range(1, NY)]
    top = jnp.maximum(jnp.maximum(stats[0], stats[1]), jnp.maximum(stats[2], stats[3]))
    raised = [jnp.exp2(s - top) for s in stats]
    whole = raised[0] + raised[1] + raised[2] + raised[3]
    shares = [r / whole for r in raised]
    for k in range(NY):
        for d in range(1, NY):
            remote(ob.at[k, yp[d]], rb.at[d, k], os.at[d, k], orr.at[d, k], y=yp[d]).wait_recv()
        pieces = [ob[k, y]] + [rb[d, k] for d in range(1, NY)]
        for h in range(2):
            head = 2 * k + h
            value = sum(
                piece[:, 128 * h : 128 * h + 128].astype(F32) * share[:, head : head + 1]
                for piece, share in zip(pieces, shares)
            )
            out[:, 128 * head : 128 * head + 128] = value.astype(BF16)

    for copy in kcopies + qcopies + [last_right, last_left]:
        copy.wait_send()

    @pl.loop(1, 4)
    def _(s):
        send_right(s).wait_send()
        send_left(s).wait_send()

    for d in range(1, NY):
        remote(sb.at[yp[d]], rsb.at[d], ss.at[d], sr.at[d], y=yp[d]).wait_send()
        for k in range(NY):
            remote(ob.at[k, yp[d]], rb.at[d, k], os.at[d, k], orr.at[d, k], y=yp[d]).wait_send()


def tables(tokens):
    inverse = 10000.0 ** (-jnp.arange(16, dtype=F32) / 16)
    row = (tokens // GRID_W).astype(F32)
    col = (tokens % GRID_W).astype(F32)
    return row, col, inverse


def on_device(
    latent_in, condition, context_latent, context_rope, shift_weight, scale_weight, gate_weight,
    norm_gain, down_query, down_latent, down_rope, query_gain, latent_gain, up_query, up_key,
    up_value, context_bias, out_weight,
):
    sp = lax.axis_index("z") * NX + lax.axis_index("x")
    own = (sp * NY + lax.axis_index("y")) * ROWS + jnp.arange(ROWS, dtype=jnp.int32)
    row, col, inverse = tables(own)
    ra, ca = row[:, None] * inverse, col[:, None] * inverse
    own_angles = jnp.concatenate([ra, ra, ca, ca], axis=1)
    row, col, inverse = tables(sp * QN + jnp.arange(QN, dtype=jnp.int32))
    ra, ca = inverse[:, None] * row, inverse[:, None] * col
    line_angles = jnp.concatenate([ra, ra, ca, ca], axis=0)

    vmem = pl.BlockSpec(memory_space=pltpu.VMEM)
    smem = pl.BlockSpec(memory_space=pltpu.SMEM)
    hbm = pl.BlockSpec(memory_space=pl.ANY)
    dma = pltpu.SemaphoreType.DMA
    shape = jax.ShapeDtypeStruct
    qlow, kblk, gate, bias, ctx, uq, uk, uv = pl.pallas_call(
        prepare_kernel,
        name="prepare",
        out_shape=(
            shape((ROWS, 512), BF16),
            shape((ROWS, 384), BF16),
            shape((1, D), F32),
            shape((NY, 128), F32),
            shape((8, 16, 384), BF16),
            shape((NY, 512, 384), BF16),
            shape((NY, 256, 256), BF16),
            shape((NY, 256, 256), BF16),
        ),
        in_specs=[vmem] * 4 + [smem] + [vmem] * 8 + [hbm] * 6,
        out_specs=(vmem,) * 8,
        scratch_shapes=[
            pltpu.VMEM((D, 512), BF16),
            pltpu.VMEM((D, 256), BF16),
            pltpu.VMEM((D, 64), BF16),
            pltpu.VMEM((NX, 3, 512), F32),
            pltpu.VMEM((NZ, 3, 512), F32),
            pltpu.VMEM((NY, 4, 512), F32),
            pltpu.VMEM((16, 384), BF16),
            pltpu.VMEM((NX, 16, 384), BF16),
            dma((3,)), dma((3,)),
            dma((NX,)), dma((NX,)),
            dma((NZ,)), dma((NZ,)),
            dma((NY,)), dma((NY,)),
            dma((NX,)), dma((NX,)),
            dma((NZ,)), dma((2,)),
            dma((NY, 3)), dma((NY, 3)),
            dma((NY, 3)), dma((NY, 3)),
        ],
        compiler_params=pltpu.CompilerParams(
            collective_id=0, has_side_effects=True, vmem_limit_bytes=48 * 1024 * 1024
        ),
    )(
        condition.reshape(1, -1), shift_weight, scale_weight, gate_weight, context_bias,
        latent_in, norm_gain.reshape(1, -1), query_gain.reshape(1, -1),
        latent_gain.reshape(1, -1), jnp.cos(own_angles), jnp.sin(own_angles),
        context_latent, context_rope, down_query, down_latent, down_rope,
        up_query, up_key, up_value,
    )
    attended = pl.pallas_call(
        attend_kernel,
        name="attend",
        out_shape=shape((ROWS, 1024), BF16),
        in_specs=[vmem] * 9,
        out_specs=vmem,
        scratch_shapes=[
            pltpu.VMEM((NY, ROWS, 512), BF16),
            pltpu.VMEM((NZ, NX, ROWS, 384), BF16),
            pltpu.VMEM((NY, 384, 512), BF16),
            pltpu.VMEM((NY, 256, 256), BF16),
            pltpu.VMEM((8, 256, QN), BF16),
            pltpu.VMEM((8, 1, QN), F32),
            pltpu.VMEM((8, 1, QN), F32),
            pltpu.VMEM((8, 128, QN), F32),
            pltpu.VMEM((NY, NY, ROWS, 256), BF16),
            pltpu.VMEM((NY, NY, ROWS, 256), BF16),
            pltpu.VMEM((8, QN), F32),
            pltpu.VMEM((NY, ROWS, 128), F32),
            pltpu.VMEM((NY, ROWS, 128), F32),
            dma((NY,)), dma((NY,)),
            dma((NX,)), dma((NX,)),
            dma((5,)), dma((5,)),
            dma((5,)), dma((5,)),
            dma((NY, NY)), dma((NY, NY)),
            dma((NY,)), dma((NY,)),
        ],
        compiler_params=pltpu.CompilerParams(
            collective_id=1, has_side_effects=True, vmem_limit_bytes=56 * 1024 * 1024
        ),
    )(qlow, kblk, uq, uk, uv, ctx, bias, jnp.cos(line_angles), jnp.sin(line_angles))
    mixed = jnp.dot(attended, out_weight, preferred_element_type=F32)
    return (latent_in.astype(F32) + gate * mixed).astype(BF16)


def solution(mesh):
    split = Mesh(mesh.devices.reshape(NZ, NX, NY, 2), ("z", "x", "y", "c"))
    rows = P(("c", "z", "x", "y"), None)
    held = P(("c", "z", "x"), None)
    weight = P(("z", "x"), "y")
    placed = (
        rows, P(("c", "z", "x")), held, held, weight, weight, weight, P(), P(), P(), P(), P(),
        P(), P(None, "y"), P(None, "y"), P(None, "y"), P("y"), P(),
    )
    return jax.shard_map(
        on_device, mesh=split, in_specs=placed, out_specs=rows, check_vma=False
    )
```

time: 260 us -> 118 us (0.45)
  blocking collectives: 128 us -> 0 us
  Pallas kernels: 0 us -> 92.5 us
  matrix products: 65.6 us -> 3.88 us
  starting transfers between devices: 16.1 us -> 0 us
  waiting for transfers between devices: 15.4 us -> 0 us
  between operations: 13.7 us -> 0.09 us
  local copies, waits for them, and re-layouts: 10.4 us -> 18.8 us
  other arithmetic: 9.4 us -> 1.36 us
    all_gather x6 -> x0, blocking collectives: 118 us -> none  [the longest x1 54.1 us: gather_packed(): lines, at, outs = (lax.all_gather(ravelled, axis), 0, [])]
    pallas_call x0 -> x2, Pallas kernels: none -> 92.5 us  [the longest x1 61.1 us: on_device(): pl.pallas_call(attend_kernel, name='attend', out_shape=shape((ROWS, 1024)...]
    dot_general x43 -> x1, matrix products: 65.6 us -> 3.88 us  [on_device(): mixed = jnp.dot(attended, out_weight, preferred_element_type=F32)]
    unnamed x26 -> x47, local copies, waits for them, and re-layouts: 0.17 us -> 18.8 us
    all_to_all x2 -> x0, starting transfers between devices: 16.1 us -> none  [copy_for_each(): return lax.all_to_all(copies, axis, split_axis=0, concat_axis=0, tiled=True)]
    all_to_all x2 -> x0, waiting for transfers between devices: 15.4 us -> none  [copy_for_each(): return lax.all_to_all(copies, axis, split_axis=0, concat_axis=0, tiled=True)]
    all_to_all x1 -> x0, blocking collectives: 10.1 us -> none  [on_device(): lax.all_to_all(attended, 'tp', split_axis=0, concat_axis=1, tiled=True)]
    reduce_sum x9 -> x0, other arithmetic: 6.69 us -> none  [the longest x7 5.45 us: attend(): new_total = run_total * shrink + jnp.sum(weights, axis=-1)]
  transfers between devices with their start and end apart: 4 -> 0, of which waited for: 2 -> 0; matrix products, arithmetic and copies ran while one was open for 8% -> 0% of each run, Pallas kernels for 0% -> 0%
where the time goes in v1:
time: 118 us; the launch traced here: 117 us
  Pallas kernels  92.5 us (78%)
  local copies, waits for them, and re-layouts  18.8 us (16%)
  matrix products  3.88 us (3%)
  other arithmetic  1.36 us (1%)
    pallas_call x1, Pallas kernels, on_device(): pl.pallas_call(attend_kernel, name='attend', out_shape=shape((ROWS, 1024)...  61.1 us
    pallas_call x1, Pallas kernels, on_device(): pl.pallas_call(prepare_kernel, name='prepare', out_shape=(shape((ROWS, 51...  31.4 us
    unnamed x47, local copies, waits for them, and re-layouts  18.8 us
    dot_general x1, matrix products, on_device(): mixed = jnp.dot(attended, out_weight, preferred_element_type=F32)  3.88 us

profile of v1, /device:TPU:2, one launch (start us, length us, event | category | flops | bytes accessed | tf_op | source)
XLA Modules:
  0.0 116.6 jit_solution(17947344492203685994)
XLA Ops:
  0.0 0.1 broadcast_multiply_fusion.1
  0.1 0.3 fusion.4
  0.4 1.2 %copy.19.dr_h = bf16[2048,64]{1,0:T(8,128)(2,1)S(1)} copy(bf16[2048,64]{0,1:T(8,128)(2,1)} %param.28) | data formatting | bytes 524288 | tf_op args[10]
  1.6 0.0 copy-start
  1.7 1.0 copy-done
  2.6 0.0 copy-start.3
  2.6 1.2 %copy-done.3 = bf16[2048,256]{1,0:T(8,128)(2,1)S(1)} copy-done((bf16[2048,256]{1,0:T(8,128)(2,1)S(1)}, bf16[2048,256]{1,0:T(8,128)(2,1)}, u32[]{:S(2)}) %copy-start.3) | copy-done | bytes 1048600
  3.9 0.0 copy-start.6
  3.9 1.0 copy-done.6
  4.9 0.0 copy-start.7
  4.9 0.9 copy-done.7
  5.8 0.0 copy-start.8
  5.8 0.9 copy-done.8
  6.7 0.0 copy-start.12
  6.7 0.8 copy-done.12
  7.5 0.0 copy-start.13
  7.5 0.8 copy-done.13
  8.4 0.0 copy-start.14
  8.4 0.8 copy-done.14
  9.2 0.0 copy-start.15
  9.2 0.7 copy-done.15
  9.9 0.0 copy-start.16
  9.9 0.7 copy-done.16
  10.6 0.0 copy-start.17
  10.6 0.7 copy-done.17
  11.3 0.0 copy-start.18
  11.3 0.7 copy-done.18
  12.0 0.0 copy-start.20
  12.0 0.7 copy-done.20
  12.6 0.0 copy-start.21
  12.6 0.7 copy-done.21
  13.3 0.0 copy-start.22
  13.3 0.7 copy-done.22
  13.9 0.0 copy-start.1
  14.0 31.4 %prepare.1 = (bf16[96,512]{1,0:T(8,128)(2,1)S(1)}, bf16[96,384]{1,0:T(8,128)(2,1)S(1)}, f32[1,2048]{1,0:T(1,128)S(1)}, f32[4,128]{1,0:T(4,128)S(1)}, bf16[8,16,3...) custom-call(bf16[1,64]{1,0:T(2,128)(2,1)S(1)} %bitcast.11, ...), custom_call_target="tpu_custom_call" | custom-call | tf_op jit(solution)/shard_map/prepare/pallas_call | solution.py:396
  45.4 0.0 copy-start.2
  45.4 1.2 %copy-done.2 = bf16[4,512,384]{2,1,0:T(8,128)(2,1)} copy-done((bf16[4,512,384]{2,1,0:T(8,128)(2,1)}, bf16[4,512,384]{2,1,0:T(8,128)(2,1)S(1)}, u32[]{:S(2)}) %copy-start.2) | copy-done | bytes 1572888
  46.6 0.0 copy-start.4
  46.6 0.8 copy-done.4
  47.4 0.0 copy-start.5
  47.4 0.8 copy-done.5
  48.2 0.0 copy-start.9
  48.2 0.6 copy-done.9
  48.8 0.0 copy-start.10
  48.8 0.6 copy-done.10
  49.4 0.0 copy-start.11
  49.4 0.6 copy-done.11
  50.1 0.0 copy-start.19
  50.1 0.6 copy-done.19
  50.7 0.1 broadcast_multiply_fusion.3
  50.7 0.9 fusion.2
  51.6 61.1 %attend.1 = bf16[96,1024]{1,0:T(8,128)(2,1)} custom-call(bf16[96,512]{1,0:T(8,128)(2,1)} %copy-done.9, bf16[96,384]{1,0:T(8,128)(2,1)} %copy-done.11, bf16[4,512,384]{2,1,0:T(8,128)(2,1)} %copy-done.2, bf16[4,256,256]{2,1,0:T(8,128)(2,1)} %copy-done.4, bf16[4,256,256]{2,1,0:T(8,128)(2,1)} %copy-done.5, bf16[8,16,384]{2,1,0:T(8,128)(2,1)} %copy-done.10, ...), custom_call_target="tpu_custom_call" | custom-call | tf_op jit(solution)/shard_map/attend/pallas_call | solution.py:439
  112.7 0.0 copy-done.1
  112.7 3.9 %fusion.1 = bf16[96,2048]{1,0:T(8,128)(2,1)} fusion(bf16[96,1024]{1,0:T(8,128)(2,1)} %attend.1, bf16[1024,2048]{1,0:T(8,128)(2,1)} %param.35, bf16[96,2048]{1,0:T(8,128)(2,1)S(1)} %copy-done.1, f32[2048]{0:T(1024)S(1)} %bitcast.8), kind=kOutput, calls=%fused_computation.2 | convolution fusion | flops 403439616 | bytes 5185536 | tf_op jit(solution)/shard_map/dot_general | solution.py:470
  (3 shorter events, 0.0 us)
Async XLA Ops:
  1.6 1.0 copy-start
  2.6 1.2 %copy-start.3 = (bf16[2048,256]{1,0:T(8,128)(2,1)S(1)}, bf16[2048,256]{1,0:T(8,128)(2,1)}, u32[]{:S(2)}) copy-start(bf16[2048,256]{1,0:T(8,128)(2,1)} %dl_h.1) | copy-start | bytes 3145732
  3.9 1.0 copy-start.6
  4.9 0.9 copy-start.7
  5.8 0.9 copy-start.8
  6.7 0.8 copy-start.12
  7.5 0.8 copy-start.13
  8.4 0.8 copy-start.14
  9.2 0.7 copy-start.15
  9.9 0.7 copy-start.16
  10.6 0.7 copy-start.17
  11.3 0.7 copy-start.18
  12.0 0.7 copy-start.20
  12.6 0.7 copy-start.21
  13.3 0.7 copy-start.22
  13.9 98.8 %copy-start.1 = (bf16[96,2048]{1,0:T(8,128)(2,1)S(1)}, bf16[96,2048]{1,0:T(8,128)(2,1)}, u32[]{:S(2)}) copy-start(bf16[96,2048]{1,0:T(8,128)(2,1)} %lat.1) | copy-start | bytes 1179652
  45.4 1.2 %copy-start.2 = (bf16[4,512,384]{2,1,0:T(8,128)(2,1)}, bf16[4,512,384]{2,1,0:T(8,128)(2,1)S(1)}, u32[]{:S(2)}) copy-start(bf16[4,512,384]{2,1,0:T(8,128)(2,1)S(1)} %get-tuple-element.16.uq) | copy-start | bytes 4718596
  46.6 0.8 copy-start.4
  47.4 0.8 copy-start.5
  48.2 0.6 copy-start.9
  48.8 0.6 copy-start.10
  49.4 0.6 copy-start.11
  50.1 0.6 copy-start.19

commit v2 on v1

v2 whole, which is shorter than its diff:
```python
import math

import jax
import jax.numpy as jnp
import numpy as np
from jax import lax
from jax.experimental import pallas as pl
from jax.experimental.pallas import tpu as pltpu
from jax.sharding import Mesh
from jax.sharding import PartitionSpec as P

ROWS = 96
D = 2048
NZ, NX, NY = 8, 4, 4
GRID_W = 64
CTXK = 128
EPS = 1e-06
QN = NY * ROWS
BUNDLE = NX * ROWS
LOG2E = math.log2(math.e)
SCALE2 = LOG2E / math.sqrt(192.0)
MESH = pl.DeviceIdType.MESH
F32 = jnp.float32
BF16 = jnp.bfloat16
NEG = float("-inf")


def dot(a, b):
    return jnp.dot(a, b, preferred_element_type=F32)


def dot_nt(a, b):
    return lax.dot_general(a, b, (((1,), (1,)), ((), ())), preferred_element_type=F32)


def remote(src, dst, send_sem, recv_sem, **where):
    return pltpu.make_async_remote_copy(
        src_ref=src, dst_ref=dst, send_sem=send_sem, recv_sem=recv_sem,
        device_id=where, device_id_type=MESH,
    )


def greet(peers):
    barrier = pltpu.get_barrier_semaphore()
    for where in peers:
        pl.semaphore_signal(barrier, inc=1, device_id=where, device_id_type=MESH)
    pl.semaphore_wait(barrier, len(peers))


def piece_order(k):
    return k + (k // 2) * (5 - 2 * k)


def kernel(
    cond_h, sw_h, cw_h, gw_h, bias_h, lat_h, gain_h, qg_h, lg_h, rowt_h, colt_h, ctxl_h, ctxr_h,
    dq_h, dl_h, dr_h, uq_h, uk_h, uv_h, ow_h,
    out,
    cond, sw, cw, gw, bias, lat, gain, qg, lg, rowt, colt, ctxl, ctxr, dq, dl, dr, ow,
    uq, uk, uv, mod_x, mod_z, mod_y, cblk, cx, ctx, kblk, qlow, gate_s, bias_s,
    qa, zk, wq_t, wv_t, q_t, kn, vt, sa, sb, m_s, l_s, acc, ob, rb, st, rst, mixed,
    in_sem, own_sem, xs, xr, zs, zr, ys, yr, cxs, cxr, czs, czr, ws, wr, hs, hr, fs, fr,
    ks, kr, qs, qr, rs, rr, ls, lr, os, orr, ss, sr,
):
    z, x, y, c = (lax.axis_index(n) for n in ("z", "x", "y", "c"))
    sp = z * NX + x
    fetches = [
        pltpu.make_async_copy(h, v, in_sem.at[i])
        for i, (h, v) in enumerate((
            (cond_h, cond), (sw_h, sw), (cw_h, cw), (gw_h, gw), (bias_h, bias), (ctxl_h, ctxl),
            (ctxr_h, ctxr), (lat_h, lat), (gain_h, gain), (qg_h, qg), (lg_h, lg),
            (rowt_h, rowt), (colt_h, colt), (dq_h, dq), (dl_h, dl), (dr_h, dr), (ow_h, ow),
        ))
    ]
    owns = [
        pltpu.make_async_copy(h, v.at[y], own_sem.at[i])
        for i, (h, v) in enumerate(((uq_h, uq), (uk_h, uk), (uv_h, uv)))
    ]
    for copy in fetches[:8] + owns + fetches[8:]:
        copy.start()
    xp = [lax.rem(x + d, NX) for d in range(NX)]
    yp = [lax.rem(y + d, NY) for d in range(NY)]
    zp = [lax.rem(z + d, NZ) for d in range(NZ)]
    right, left = zp[1], zp[NZ - 1]
    greet(
        [{"x": xp[d]} for d in range(1, NX)]
        + [{"y": yp[d]} for d in range(1, NY)]
        + [{"z": zp[d]} for d in range(1, NZ)]
        + [{"c": 1 - c}]
    )

    for copy in fetches[:7]:
        copy.wait()
    v = cond[...].astype(F32)
    activated = (v / (1.0 + jnp.exp(-v))).astype(BF16)
    mod_x[x] = jnp.concatenate([dot(activated, w[...]) for w in (sw, cw, gw)], axis=0)
    xcopies = [
        remote(mod_x.at[x], mod_x.at[x], xs.at[d], xr.at[d], x=xp[d]) for d in range(1, NX)
    ]
    for copy in xcopies:
        copy.start()
    cblk[...] = jnp.concatenate([ctxl[...], ctxr[...], jnp.zeros((16, 64), BF16)], axis=1)
    cx[x] = cblk[...]
    ccopies = [remote(cblk, cx.at[x], cxs.at[d], cxr.at[d], x=xp[d]) for d in range(1, NX)]
    for copy in ccopies:
        copy.start()

    for copy in owns:
        copy.wait()

    def half(ref, slot):
        rows = ref.shape[1] // 2
        return ref.at[slot, pl.ds(pl.multiple_of(c * rows, rows), rows)]

    ups = (uq, uk, uv)
    after = [
        remote(half(w, y), half(w, y), ws.at[0, i], wr.at[0, i], y=yp[1])
        for i, w in enumerate(ups)
    ]
    before = [
        remote(half(w, y), half(w, y), ws.at[1, i], wr.at[1, i], y=yp[3])
        for i, w in enumerate(ups)
    ]
    hops = [
        remote(half(uq, yp[3]), half(uq, yp[3]), hs.at[0], hr.at[0], y=yp[1]),
        remote(half(uk, yp[1]), half(uk, yp[1]), hs.at[1], hr.at[1], y=yp[3]),
        remote(half(uv, yp[1]), half(uv, yp[1]), hs.at[2], hr.at[2], y=yp[3]),
    ]

    def across(slot, d, i):
        return remote(half(ups[i], slot), half(ups[i], slot), fs.at[d, i], fr.at[d, i], c=1 - c)

    after[0].start()
    before[0].start()
    after[1].start()
    before[1].start()

    for copy in xcopies:
        copy.wait_recv()
    mod_z[z] = mod_x[0] + mod_x[1] + mod_x[2] + mod_x[3]
    zcopies = [
        remote(mod_z.at[z], mod_z.at[z], zs.at[d], zr.at[d], z=zp[d]) for d in range(1, NZ)
    ]
    for copy in zcopies:
        copy.start()
    for copy in fetches[7:13]:
        copy.wait()
    lat32 = lat[...].astype(F32)
    inv = lax.rsqrt(jnp.mean(lat32 * lat32, axis=-1, keepdims=True) + EPS)
    scaled = lat32 * inv * gain[...]
    line = [rowt[pl.ds(sp * 6 + i, 1), :] + colt[...] for i in range(6)]
    line_t = jnp.concatenate(line, axis=0).T
    own_table = []
    for t in range(3):
        g = y * 3 + t
        own_table.append(
            rowt[pl.ds(sp * 6 + g // 2, 1), :]
            + colt[pl.ds(pl.multiple_of((g % 2) * 32, 32), 32), :]
        )
    own_table = jnp.concatenate(own_table, axis=0)
    wq_t[y] = uq[y].T
    wv_t[y] = uv[y].T
    m_s[...] = jnp.full(m_s.shape, NEG, F32)
    l_s[...] = jnp.zeros(l_s.shape, F32)
    acc[...] = jnp.zeros(acc.shape, F32)
    for copy in ccopies:
        copy.wait_recv()
    mine = z // 2 == y
    zc = [
        remote(
            cx, ctx.at[pl.ds(pl.multiple_of((z % 2) * NX, NX), NX)], czs.at[d],
            czr.at[z % 2], z=zp[d],
        )
        for d in range(1, NZ)
    ]

    @pl.when(mine)
    def _():
        ctx[pl.ds((z % 2) * NX, NX)] = cx[...]
        for copy in zc:
            copy.start()

    for copy in zcopies:
        copy.wait_recv()
    total = mod_z[0]
    for k in range(1, NZ):
        total = total + mod_z[k]
    bias_row = jnp.concatenate([bias[...], jnp.zeros((1, 510), F32)], axis=1)
    mod_y[y] = jnp.concatenate([total, bias_row], axis=0)
    ycopies = [
        remote(mod_y.at[y], mod_y.at[y], ys.at[d], yr.at[d], y=yp[d]) for d in range(1, NY)
    ]
    for copy in ycopies:
        copy.start()
    after[0].wait_recv()
    hops[0].start()
    across(yp[3], 0, 0).start()
    before[0].wait_recv()
    across(yp[1], 1, 0).start()
    before[1].wait_recv()
    hops[1].start()
    across(yp[1], 1, 1).start()
    after[1].wait_recv()
    across(yp[3], 0, 1).start()
    before[2].start()
    after[2].start()

    for copy in ycopies:
        copy.wait_recv()
    shift = jnp.concatenate([mod_y[k, 0:1] for k in range(NY)], axis=1)
    scale = jnp.concatenate([mod_y[k, 1:2] for k in range(NY)], axis=1)
    gate_s[...] = jnp.concatenate([mod_y[k, 2:3] for k in range(NY)], axis=1)
    bias_s[...] = jnp.concatenate([mod_y[k, 3:4, 0:128] for k in range(NY)], axis=0)
    normed = (scaled * (1.0 + scale) + shift).astype(BF16)
    for copy in fetches[13:16]:
        copy.wait()

    def rms(a, g):
        return a * lax.rsqrt(jnp.mean(a * a, axis=-1, keepdims=True) + EPS) * g

    low = rms(dot(normed, dl[...]), lg[...]).astype(BF16)
    u = dot_nt(normed, dr[...])
    turned = jnp.concatenate([-u[:, 16:32], u[:, 0:16], -u[:, 48:64], u[:, 32:48]], axis=1)
    rope = (u * own_table[:, :64] + turned * own_table[:, 64:]).astype(BF16)
    kblk[...] = jnp.concatenate([low, rope, jnp.zeros((ROWS, 64), BF16)], axis=1)
    zk[z, x] = kblk[...]
    kcopies = [remote(kblk, zk.at[z, x], ks.at[d], kr.at[d], x=xp[d]) for d in range(1, NX)]

    def slot_of(offset):
        return lax.rem(z + offset + NZ, NZ)

    def piece(offset, j):
        return zk.at[slot_of(offset), lax.rem(x - piece_order(j) + NX, NX)]

    def go_right(s, j):
        return remote(piece(1 - s, j), piece(1 - s, j), rs.at[s, j], rr.at[s, j], z=right)

    def go_left(s, j):
        return remote(piece(s - 1, j), piece(s - 1, j), ls.at[s, j], lr.at[s, j], z=left)

    for copy in kcopies:
        copy.start()
    go_right(1, 0).start()
    go_left(1, 0).start()
    qlow[...] = rms(dot(normed, dq[...]), qg[...]).astype(BF16)
    qcopies = [remote(qlow, qa.at[y], qs.at[d], qr.at[d], y=yp[d]) for d in range(1, NY)]
    for copy in qcopies:
        copy.start()
    qa[y] = qlow[...]

    before[2].wait_recv()
    hops[2].start()
    across(yp[1], 1, 2).start()
    after[2].wait_recv()
    across(yp[3], 0, 2).start()
    for i in range(3):
        hops[i].wait_recv()
        across(yp[2], 2, i).start()
    for j, d in ((1, 1), (2, 3), (3, 2)):
        kcopies[d - 1].wait_recv()
        go_right(1, j).start()
        go_left(1, j).start()
    for d, slot in ((0, yp[3]), (1, yp[1]), (2, yp[2])):
        for i in range(3):
            across(slot, d, i).wait_recv()
        wq_t[slot] = uq[slot].T
        wv_t[slot] = uv[slot].T
    for k in range(2):
        @pl.when(z != 2 * y + k)
        def _():
            remote(cx, ctx.at[pl.ds(k * NX, NX)], czs.at[0], czr.at[k], z=zp[1]).wait_recv()

    for copy in qcopies:
        copy.wait_recv()

    @pl.loop(0, NY)
    def _(k):
        qt = dot_nt(wq_t[k], qa[...].reshape(QN, 512))
        for h in range(2):
            b = 192 * h
            u = qt[b + 128 : b + 192]
            turned = jnp.concatenate([-u[16:32], u[0:16], -u[48:64], u[32:48]], axis=0)
            rope = u * line_t[:64] + turned * line_t[64:]
            q_t[k, h] = jnp.concatenate(
                [qt[b : b + 128], rope, jnp.zeros((64, QN), F32)], axis=0
            ).astype(BF16)

    def softmax(s_ref, n, k, h, biased):
        top = jnp.max(s_ref[0:n], axis=0, keepdims=True) * SCALE2
        lift = bias_s[pl.ds(k, 1), h : h + 1] * LOG2E if biased else None
        m_old = m_s[k, h]
        m_new = jnp.maximum(m_old, top + lift if biased else top)
        p = jnp.exp2(s_ref[0:n] * SCALE2 - (m_new - lift if biased else m_new))
        shrink = jnp.exp2(m_old - m_new)
        l_s[k, h] = l_s[k, h] * shrink + jnp.sum(p, axis=0, keepdims=True)
        m_s[k, h] = m_new
        return p.astype(BF16), shrink

    def process(n, load, biased, hook, finish=None):
        def project(k):
            low = load()[:, :256]
            return dot(low, uk[k]).astype(BF16), dot_nt(wv_t[k], low).astype(BF16)

        def score(nope, h, k):
            key = jnp.concatenate([nope[:, 128 * h : 128 * h + 128], load()[:, 256:]], axis=1)
            return dot(key, q_t[k, h])

        def step(k, final):
            hook(k)
            now = kn[0:n]
            sb[0:n] = score(now, 1, k)
            if not final:
                nope, val = project(k + 1)
            p, shrink = softmax(sa, n, k, 0, biased)
            acc[k, 0] = acc[k, 0] * shrink + dot(vt[0:128, 0:n], p)
            if not final:
                sa[0:n] = score(nope, 0, k + 1)
            p, shrink = softmax(sb, n, k, 1, biased)
            acc[k, 1] = acc[k, 1] * shrink + dot(vt[128:256, 0:n], p)
            if not final:
                kn[0:n] = nope
                vt[:, 0:n] = val
            if finish is not None:
                finish(k)

        nope, val = project(0)
        kn[0:n] = nope
        vt[:, 0:n] = val
        sa[0:n] = score(nope, 0, 0)

        @pl.loop(0, NY - 1)
        def _(k):
            step(k, False)

        step(NY - 1, True)

    def nothing(k):
        pass

    def pass_on(s):
        def hook(k):
            go_right(s, k).wait_recv()
            go_left(s, k).wait_recv()
            go_right(s + 1, k).start()
            go_left(s + 1, k).start()

        return hook

    def pass_last(k):
        go_right(3, k).wait_recv()
        go_left(3, k).wait_recv()

        @pl.when(k < 2)
        def _():
            go_right(4, k).start()

        @pl.when(k >= 2)
        def _():
            go_left(4, k).start()

    def bundle(offset):
        return zk[slot_of(offset)].reshape(BUNDLE, 384)

    def around(s):
        return lambda: jnp.concatenate([bundle(-s), bundle(s)], axis=0)

    def out_copy(k, d):
        return remote(ob.at[k, yp[d]], rb.at[d, k], os.at[d, k], orr.at[d, k], y=yp[d])

    def finish(k):
        both = []
        for h in range(2):
            total = l_s[k, h]
            both.append((acc[k, h] / total).T)
            row = m_s[k, h] + jnp.log2(total)
            for j in range(NY):
                st[j, k, h : h + 1] = jnp.concatenate(
                    [row[:, ROWS * j : ROWS * j + ROWS], jnp.zeros((1, 32), F32)], axis=1
                )
        ob[k] = jnp.concatenate(both, axis=1).astype(BF16).reshape(NY, ROWS, 256)
        for d in range(1, NY):
            out_copy(k, d).start()

    process(CTXK, lambda: ctx[...].reshape(CTXK, 384), True, nothing)
    process(BUNDLE, lambda: bundle(0), False, pass_on(1))
    process(2 * BUNDLE, around(1), False, pass_on(2))
    process(2 * BUNDLE, around(2), False, pass_last)
    for j in range(2):
        go_right(4, j).wait_recv()
        go_left(4, j + 2).wait_recv()
    process(
        3 * BUNDLE,
        lambda: jnp.concatenate([bundle(-3), bundle(3), bundle(4)], axis=0),
        False, nothing, finish,
    )

    def stat_copy(d):
        return remote(st.at[yp[d]], rst.at[d], ss.at[d], sr.at[d], y=yp[d])

    for d in range(1, NY):
        stat_copy(d).start()
    for d in range(1, NY):
        stat_copy(d).wait_recv()
    stats = [st[y]] + [rst[d] for d in range(1, NY)]
    top = jnp.maximum(jnp.maximum(stats[0], stats[1]), jnp.maximum(stats[2], stats[3]))
    raised = [jnp.exp2(s - top) for s in stats]
    whole = raised[0] + raised[1] + raised[2] + raised[3]
    fill = jnp.zeros((120, 128), F32)
    shares = [
        jnp.concatenate([(r / whole).reshape(8, 128), fill], axis=0).T[:ROWS] for r in raised
    ]
    fetches[16].wait()
    for k in range(NY):
        for d in range(1, NY):
            out_copy(k, d).wait_recv()
        pieces = [ob[k, y]] + [rb[d, k] for d in range(1, NY)]
        both = []
        for h in range(2):
            head = 2 * k + h
            both.append(sum(
                p[:, 128 * h : 128 * h + 128].astype(F32) * share[:, head : head + 1]
                for p, share in zip(pieces, shares)
            ))
        part = dot(jnp.concatenate(both, axis=1).astype(BF16), ow[256 * k : 256 * k + 256])
        if k == 0:
            mixed[...] = part
        elif k < NY - 1:
            mixed[...] += part
        else:
            out[...] = (
                lat[...].astype(F32) + gate_s[...] * (mixed[...] + part)
            ).astype(BF16)

    for copy in xcopies + ccopies + zcopies + ycopies + after + before + hops + kcopies + qcopies:
        copy.wait_send()

    @pl.when(mine)
    def _():
        for copy in zc:
            copy.wait_send()

    for d in range(3):
        for i in range(3):
            across(yp[d], d, i).wait_send()
    for j in range(NX):
        for s in range(1, 4):
            go_right(s, j).wait_send()
            go_left(s, j).wait_send()
        if j < 2:
            go_right(4, j).wait_send()
        else:
            go_left(4, j).wait_send()
    for d in range(1, NY):
        stat_copy(d).wait_send()
        for k in range(NY):
            out_copy(k, d).wait_send()


def rope_constants():
    inverse = (10000.0 ** (-np.arange(16, dtype=np.float64) / 16)).astype(np.float32)

    def spread(count, first):
        angles = (np.arange(count, dtype=np.float32)[:, None] * inverse).astype(np.float64)
        zero = np.zeros((count, 32))
        runs = []
        for f in (np.cos, np.sin):
            pair = np.concatenate([f(angles), f(angles)], axis=1)
            runs += [pair, zero] if first else [zero, pair]
        return np.concatenate(runs, axis=1).astype(np.float32)

    return spread(192, True), spread(GRID_W, False)


def on_device(
    latent_in, condition, context_latent, context_rope, shift_weight, scale_weight, gate_weight,
    norm_gain, down_query, down_latent, down_rope, query_gain, latent_gain, up_query, up_key,
    up_value, context_bias, out_weight,
):
    row_table, col_table = rope_constants()
    vmem = pltpu.VMEM
    dma = pltpu.SemaphoreType.DMA
    return pl.pallas_call(
        kernel,
        name="whole",
        out_shape=jax.ShapeDtypeStruct((ROWS, D), BF16),
        in_specs=[pl.BlockSpec(memory_space=pltpu.HBM)] * 20,
        out_specs=pl.BlockSpec(memory_space=pltpu.VMEM),
        scratch_shapes=[
            vmem((1, 64), BF16),
            vmem((64, 512), BF16), vmem((64, 512), BF16), vmem((64, 512), BF16),
            vmem((1, 2), F32),
            vmem((ROWS, D), BF16),
            vmem((1, D), F32), vmem((1, 512), F32), vmem((1, 256), F32),
            vmem((192, 128), F32), vmem((GRID_W, 128), F32),
            vmem((16, 256), BF16), vmem((16, 64), BF16),
            vmem((D, 512), BF16), vmem((D, 256), BF16), vmem((64, D), BF16),
            vmem((1024, D), BF16),
            vmem((NY, 512, 384), BF16), vmem((NY, 256, 256), BF16), vmem((NY, 256, 256), BF16),
            vmem((NX, 3, 512), F32), vmem((NZ, 3, 512), F32), vmem((NY, 4, 512), F32),
            vmem((16, 384), BF16), vmem((NX, 16, 384), BF16), vmem((8, 16, 384), BF16),
            vmem((ROWS, 384), BF16), vmem((ROWS, 512), BF16),
            vmem((1, D), F32), vmem((NY, 128), F32),
            vmem((NY, ROWS, 512), BF16),
            vmem((NZ, NX, ROWS, 384), BF16),
            vmem((NY, 384, 512), BF16), vmem((NY, 256, 256), BF16),
            vmem((NY, 2, 256, QN), BF16),
            vmem((3 * BUNDLE, 256), BF16), vmem((256, 3 * BUNDLE), BF16),
            vmem((3 * BUNDLE, QN), F32), vmem((3 * BUNDLE, QN), F32),
            vmem((NY, 2, 1, QN), F32), vmem((NY, 2, 1, QN), F32),
            vmem((NY, 2, 128, QN), F32),
            vmem((NY, NY, ROWS, 256), BF16), vmem((NY, NY, ROWS, 256), BF16),
            vmem((NY, NY, 2, 128), F32), vmem((NY, NY, 2, 128), F32),
            vmem((ROWS, D), F32),
            dma((17,)), dma((3,)),
            dma((NX,)), dma((NX,)),
            dma((NZ,)), dma((NZ,)),
            dma((NY,)), dma((NY,)),
            dma((NX,)), dma((NX,)),
            dma((NZ,)), dma((2,)),
            dma((2, 3)), dma((2, 3)),
            dma((3,)), dma((3,)),
            dma((3, 3)), dma((3, 3)),
            dma((NX,)), dma((NX,)),
            dma((NY,)), dma((NY,)),
            dma((5, NX)), dma((5, NX)),
            dma((5, NX)), dma((5, NX)),
            dma((NY, NY)), dma((NY, NY)),
            dma((NY,)), dma((NY,)),
        ],
        compiler_params=pltpu.CompilerParams(
            collective_id=0, has_side_effects=True, vmem_limit_bytes=60 * 1024 * 1024
        ),
    )(
        condition.reshape(1, -1), shift_weight, scale_weight, gate_weight,
        context_bias.reshape(1, -1), latent_in, norm_gain.reshape(1, -1),
        query_gain.reshape(1, -1), latent_gain.reshape(1, -1), jnp.asarray(row_table),
        jnp.asarray(col_table), context_latent, context_rope, down_query, down_latent,
        down_rope.T, up_query, up_key, up_value, out_weight,
    )


def solution(mesh):
    split = Mesh(mesh.devices.reshape(NZ, NX, NY, 2), ("z", "x", "y", "c"))
    rows = P(("c", "z", "x", "y"), None)
    held = P(("c", "z", "x"), None)
    weight = P(("z", "x"), "y")
    placed = (
        rows, P(("c", "z", "x")), held, held, weight, weight, weight, P(), P(), P(), P(), P(),
        P(), P(None, "y"), P(None, "y"), P(None, "y"), P("y"), P(),
    )
    return jax.shard_map(
        on_device, mesh=split, in_specs=placed, out_specs=rows, check_vma=False
    )
```

time: 118 us -> 73.8 us (0.63)
  the two profiles are of different devices: /device:TPU:2 before, /device:TPU:1 now
where the time goes in v2:
time: 73.8 us; the launch traced here: 73.7 us
  Pallas kernels  71.9 us (97%)
  local copies, waits for them, and re-layouts  1.77 us (2%)
    pallas_call x1, Pallas kernels, on_device(): pl.pallas_call(kernel, name='whole', out_shape=jax.ShapeDtypeStruct((ROWS...  71.9 us
    unnamed x1, local copies, waits for them, and re-layouts  1.77 us

profile of v2, /device:TPU:1, one launch (start us, length us, event | category | flops | bytes accessed | tf_op | source)
XLA Modules:
  0.0 73.7 jit_solution(4636911224034825236)
XLA Ops:
  0.0 71.9 %whole.1 = bf16[96,2048]{1,0:T(8,128)(2,1)} custom-call(bf16[1,64]{1,0:T(2,128)(2,1)} %bitcast.10, bf16[64,512]{1,0:T(8,128)(2,1)} %sw_h.1, bf16[64,512]{1,0:T(8,128)(2,1)} %cw_h.1, bf16[64,512]{1,0:T(8,128)(2,1)} %gw_h.1, f32[1,2]{1,0:T(1,128)} %bitcast.11, bf16[96,2048]{1,0:T(8,128)(2,1)} %lat_h.1, f32[1,2048]{1,0:T(1,128)} %bitcast.7, f32[1,512]{1,0:T(1,128)} %bitcast.8, ...), custom_call_target="tpu_custom_call" | custom-call | tf_op jit(solution)/shard_map/whole/pallas_call | solution.py:481
  71.9 1.8 %copy.22 = bf16[96,2048]{1,0:T(8,128)(2,1)} copy(bf16[96,2048]{1,0:T(8,128)(2,1)} %whole.1) | data formatting | bytes 786432

commit v3 on v2

--- a/solution.py
+++ b/solution.py
@@ -16,7 +16,10 @@
 CTXK = 128
 EPS = 1e-06
 QN = NY * ROWS
-BUNDLE = NX * ROWS
+ROWS_A, ROWS_B = 64, 32
+PIECE_A, PIECE_B = ROWS_A + 16, ROWS_B + 16
+BUNDLE = NX * ROWS_A
+LAST = 3 * BUNDLE + (NX - 1) * NZ * ROWS_B
 LOG2E = math.log2(math.e)
 SCALE2 = LOG2E / math.sqrt(192.0)
 MESH = pl.DeviceIdType.MESH
@@ -40,11 +43,8 @@
     )
 
 
-def greet(peers):
-    barrier = pltpu.get_barrier_semaphore()
-    for where in peers:
-        pl.semaphore_signal(barrier, inc=1, device_id=where, device_id_type=MESH)
-    pl.semaphore_wait(barrier, len(peers))
+def lane_pair(run):
+    return jnp.concatenate([run[:, 64:], run[:, :64]], axis=1)
 
 
 def piece_order(k):
@@ -56,10 +56,10 @@
     dq_h, dl_h, dr_h, uq_h, uk_h, uv_h, ow_h,
     out,
     cond, sw, cw, gw, bias, lat, gain, qg, lg, rowt, colt, ctxl, ctxr, dq, dl, dr, ow,
-    uq, uk, uv, mod_x, mod_z, mod_y, cblk, cx, ctx, kblk, qlow, gate_s, bias_s,
-    qa, zk, wq_t, wv_t, q_t, kn, vt, sa, sb, m_s, l_s, acc, ob, rb, st, rst, mixed,
-    in_sem, own_sem, xs, xr, zs, zr, ys, yr, cxs, cxr, czs, czr, ws, wr, hs, hr, fs, fr,
-    ks, kr, qs, qr, rs, rr, ls, lr, os, orr, ss, sr,
+    uq, uk, uv, mod_x, mod_z, mod_y, cblk, cx, ctx, qlow, gate_s, bias_s,
+    qa, zka, zkb, wq_t, wv_t, q_t, lows, ropes, kn, vt, sa, sb, m_s, l_s, acc, ob, rb, st, rst, mixed,
+    in_sem, own_sem, xs, xr, zs, zr, ys, yr, cxs, cxr, czs, czr, ws, wr, hs, hr, es, er, fs, fr,
+    ks, kr, bs, br, js, jr, qs, qr, rs, rr, ls, lr, os, orr, ss, sr,
 ):
     z, x, y, c = (lax.axis_index(n) for n in ("z", "x", "y", "c"))
     sp = z * NX + x
@@ -81,18 +81,24 @@
     yp = [lax.rem(y + d, NY) for d in range(NY)]
     zp = [lax.rem(z + d, NZ) for d in range(NZ)]
     right, left = zp[1], zp[NZ - 1]
-    greet(
+    peers = (
         [{"x": xp[d]} for d in range(1, NX)]
         + [{"y": yp[d]} for d in range(1, NY)]
         + [{"z": zp[d]} for d in range(1, NZ)]
         + [{"c": 1 - c}]
     )
+    barrier = pltpu.get_barrier_semaphore()
+    for where in peers:
+        pl.semaphore_signal(barrier, inc=1, device_id=where, device_id_type=MESH)
 
     for copy in fetches[:7]:
         copy.wait()
     v = cond[...].astype(F32)
     activated = (v / (1.0 + jnp.exp(-v))).astype(BF16)
     mod_x[x] = jnp.concatenate([dot(activated, w[...]) for w in (sw, cw, gw)], axis=0)
+    for copy in owns:
+        copy.wait()
+    pl.semaphore_wait(barrier, len(peers))
     xcopies = [
         remote(mod_x.at[x], mod_x.at[x], xs.at[d], xr.at[d], x=xp[d]) for d in range(1, NX)
     ]
@@ -104,35 +110,34 @@
     for copy in ccopies:
         copy.start()
 
-    for copy in owns:
-        copy.wait()
-
     def half(ref, slot):
         rows = ref.shape[1] // 2
         return ref.at[slot, pl.ds(pl.multiple_of(c * rows, rows), rows)]
 
+    def eighth(slot):
+        return uq.at[slot, pl.ds(pl.multiple_of(c * 256 + x * 64, 64), 64)]
+
+    def over_y(d, i):
+        return remote(half(ups[i], y), half(ups[i], y), ws.at[d, i], wr.at[d, i], y=yp[d])
+
+    def eighth_over_y(d):
+        return remote(eighth(y), eighth(y), hs.at[d], hr.at[d], y=yp[d])
+
+    def eighth_over_x(d, e):
+        slot = yp[NY - d]
+        return remote(eighth(slot), eighth(slot), es.at[d, e], er.at[d, e], x=xp[e])
+
+    def across(d, i):
+        slot = yp[NY - d]
+        return remote(half(ups[i], slot), half(ups[i], slot), fs.at[d, i], fr.at[d, i], c=1 - c)
+
     ups = (uq, uk, uv)
-    after = [
-        remote(half(w, y), half(w, y), ws.at[0, i], wr.at[0, i], y=yp[1])
-        for i, w in enumerate(ups)
-    ]
-    before = [
-        remote(half(w, y), half(w, y), ws.at[1, i], wr.at[1, i], y=yp[3])
-        for i, w in enumerate(ups)
-    ]
-    hops = [
-        remote(half(uq, yp[3]), half(uq, yp[3]), hs.at[0], hr.at[0], y=yp[1]),
-        remote(half(uk, yp[1]), half(uk, yp[1]), hs.at[1], hr.at[1], y=yp[3]),
-        remote(half(uv, yp[1]), half(uv, yp[1]), hs.at[2], hr.at[2], y=yp[3]),
-    ]
-
-    def across(slot, d, i):
-        return remote(half(ups[i], slot), half(ups[i], slot), fs.at[d, i], fr.at[d, i], c=1 - c)
-
-    after[0].start()
-    before[0].start()
-    after[1].start()
-    before[1].start()
+    nearest = (1, 3, 2)
+    for d in nearest:
+        eighth_over_y(d).start()
+    for i in (1, 2):
+        for d in nearest:
+            over_y(d, i).start()
 
     for copy in xcopies:
         copy.wait_recv()
@@ -179,6 +184,11 @@
         for copy in zc:
             copy.start()
 
+    for d in nearest:
+        eighth_over_y(d).wait_recv()
+        for e in nearest:
+            eighth_over_x(d, e).start()
+
     for copy in zcopies:
         copy.wait_recv()
     total = mod_z[0]
@@ -191,18 +201,10 @@
     ]
     for copy in ycopies:
         copy.start()
-    after[0].wait_recv()
-    hops[0].start()
-    across(yp[3], 0, 0).start()
-    before[0].wait_recv()
-    across(yp[1], 1, 0).start()
-    before[1].wait_recv()
-    hops[1].start()
-    across(yp[1], 1, 1).start()
-    after[1].wait_recv()
-    across(yp[3], 0, 1).start()
-    before[2].start()
-    after[2].start()
+    for i in (1, 2):
+        for d in nearest:
+            over_y(d, i).wait_recv()
+            across(d, i).start()
 
     for copy in ycopies:
         copy.wait_recv()
@@ -217,19 +219,31 @@
     def rms(a, g):
         return a * lax.rsqrt(jnp.mean(a * a, axis=-1, keepdims=True) + EPS) * g
 
+    qlow[...] = rms(dot(normed, dq[...]), qg[...]).astype(BF16)
+    qcopies = [remote(qlow, qa.at[y], qs.at[d], qr.at[d], y=yp[d]) for d in range(1, NY)]
+    for copy in qcopies:
+        copy.start()
     low = rms(dot(normed, dl[...]), lg[...]).astype(BF16)
     u = dot_nt(normed, dr[...])
     turned = jnp.concatenate([-u[:, 16:32], u[:, 0:16], -u[:, 48:64], u[:, 32:48]], axis=1)
-    rope = (u * own_table[:, :64] + turned * own_table[:, 64:]).astype(BF16)
-    kblk[...] = jnp.concatenate([low, rope, jnp.zeros((ROWS, 64), BF16)], axis=1)
-    zk[z, x] = kblk[...]
-    kcopies = [remote(kblk, zk.at[z, x], ks.at[d], kr.at[d], x=xp[d]) for d in range(1, NX)]
+    rope = u * own_table[:, :64] + turned * own_table[:, 64:]
+    runs = [rope[16 * g : 16 * g + 16] for g in range(6)]
+    zka[z, x] = jnp.concatenate(
+        [low[:ROWS_A], jnp.concatenate(runs[:4], axis=1).astype(BF16)], axis=0
+    )
+    zkb[x, z] = jnp.concatenate(
+        [
+            low[ROWS_A:],
+            jnp.concatenate(runs[4:] + [jnp.zeros((16, 128), F32)], axis=1).astype(BF16),
+        ],
+        axis=0,
+    )
 
     def slot_of(offset):
         return lax.rem(z + offset + NZ, NZ)
 
     def piece(offset, j):
-        return zk.at[slot_of(offset), lax.rem(x - piece_order(j) + NX, NX)]
+        return zka.at[slot_of(offset), lax.rem(x - piece_order(j) + NX, NX)]
 
     def go_right(s, j):
         return remote(piece(1 - s, j), piece(1 - s, j), rs.at[s, j], rr.at[s, j], z=right)
@@ -237,31 +251,33 @@
     def go_left(s, j):
         return remote(piece(s - 1, j), piece(s - 1, j), ls.at[s, j], lr.at[s, j], z=left)
 
+    kcopies = [
+        remote(zka.at[z, x], zka.at[z, x], ks.at[d], kr.at[d], x=xp[d]) for d in range(1, NX)
+    ]
+    bcopies = [
+        remote(zkb.at[x, z], zkb.at[x, z], bs.at[d], br.at[d], z=zp[d]) for d in range(1, NZ)
+    ]
+    lines = [remote(zkb.at[x], zkb.at[x], js.at[d], jr.at[d], x=xp[d]) for d in range(1, NX)]
     for copy in kcopies:
         copy.start()
     go_right(1, 0).start()
     go_left(1, 0).start()
-    qlow[...] = rms(dot(normed, dq[...]), qg[...]).astype(BF16)
-    qcopies = [remote(qlow, qa.at[y], qs.at[d], qr.at[d], y=yp[d]) for d in range(1, NY)]
-    for copy in qcopies:
+    for copy in bcopies:
         copy.start()
     qa[y] = qlow[...]
 
-    before[2].wait_recv()
-    hops[2].start()
-    across(yp[1], 1, 2).start()
-    after[2].wait_recv()
-    across(yp[3], 0, 2).start()
-    for i in range(3):
-        hops[i].wait_recv()
-        across(yp[2], 2, i).start()
+    for d in nearest:
+        for e in nearest:
+            eighth_over_x(d, e).wait_recv()
+        across(d, 0).start()
     for j, d in ((1, 1), (2, 3), (3, 2)):
         kcopies[d - 1].wait_recv()
         go_right(1, j).start()
         go_left(1, j).start()
-    for d, slot in ((0, yp[3]), (1, yp[1]), (2, yp[2])):
-        for i in range(3):
-            across(slot, d, i).wait_recv()
+    for d in nearest:
+        for i in (1, 2, 0):
+            across(d, i).wait_recv()
+        slot = yp[NY - d]
         wq_t[slot] = uq[slot].T
         wv_t[slot] = uv[slot].T
     for k in range(2):
@@ -295,17 +311,28 @@
         m_s[k, h] = m_new
         return p.astype(BF16), shrink
 
-    def process(n, load, biased, hook, finish=None):
+    def pass_on(s, j):
+        go_right(s, j).wait_recv()
+        go_left(s, j).wait_recv()
+        if s < 3 or j < 2:
+            go_right(s + 1, j).start()
+        if s < 3 or j >= 2:
+            go_left(s + 1, j).start()
+
+    def process(n, stage, biased, passes, finish=None):
         def project(k):
-            low = load()[:, :256]
-            return dot(low, uk[k]).astype(BF16), dot_nt(wv_t[k], low).astype(BF16)
+            return dot(lows[0:n], uk[k]).astype(BF16), dot_nt(wv_t[k], lows[0:n]).astype(BF16)
 
         def score(nope, h, k):
-            key = jnp.concatenate([nope[:, 128 * h : 128 * h + 128], load()[:, 256:]], axis=1)
+            key = jnp.concatenate([nope[:, 128 * h : 128 * h + 128], ropes[0:n]], axis=1)
             return dot(key, q_t[k, h])
 
         def step(k, final):
-            hook(k)
+            for at, s, j in passes:
+                if final and at == NY - 1:
+                    pass_on(s, j)
+                elif not final and at < NY - 1:
+                    pl.when(k == at)(lambda s=s, j=j: pass_on(s, j))
             now = kn[0:n]
             sb[0:n] = score(now, 1, k)
             if not final:
@@ -322,6 +349,7 @@
             if finish is not None:
                 finish(k)
 
+        stage()
         nope, val = project(0)
         kn[0:n] = nope
         vt[:, 0:n] = val
@@ -333,35 +361,28 @@
 
         step(NY - 1, True)
 
-    def nothing(k):
-        pass
-
-    def pass_on(s):
-        def hook(k):
-            go_right(s, k).wait_recv()
-            go_left(s, k).wait_recv()
-            go_right(s + 1, k).start()
-            go_left(s + 1, k).start()
-
-        return hook
-
-    def pass_last(k):
-        go_right(3, k).wait_recv()
-        go_left(3, k).wait_recv()
-
-        @pl.when(k < 2)
-        def _():
-            go_right(4, k).start()
-
-        @pl.when(k >= 2)
-        def _():
-            go_left(4, k).start()
-
-    def bundle(offset):
-        return zk[slot_of(offset)].reshape(BUNDLE, 384)
-
-    def around(s):
-        return lambda: jnp.concatenate([bundle(-s), bundle(s)], axis=0)
+    def stage_context():
+        both = ctx[...].reshape(CTXK, 384)
+        lows[0:CTXK] = both[:, :256]
+        ropes[0:CTXK] = both[:, 256:]
+
+    def stage_a(at, offset):
+        slot = slot_of(offset)
+        lows[at : at + BUNDLE] = zka[slot, :, :ROWS_A].reshape(BUNDLE, 256)
+        for i in range(NX):
+            run = zka[slot, i, ROWS_A:]
+            for g in range(4):
+                tile = run[:, 128 * (g // 2) : 128 * (g // 2) + 128]
+                first = at + ROWS_A * i + 16 * g
+                ropes[first : first + 16] = lane_pair(tile) if g % 2 else tile
+
+    def stage_b(at, line):
+        lows[at : at + NZ * ROWS_B] = zkb[line, :, :ROWS_B].reshape(NZ * ROWS_B, 256)
+        for i in range(NZ):
+            tile = zkb[line, i, ROWS_B:, :128]
+            first = at + ROWS_B * i
+            ropes[first : first + 16] = tile
+            ropes[first + 16 : first + 32] = lane_pair(tile)
 
     def out_copy(k, d):
         return remote(ob.at[k, yp[d]], rb.at[d, k], os.at[d, k], orr.at[d, k], y=yp[d])
@@ -380,18 +401,38 @@
         for d in range(1, NY):
             out_copy(k, d).start()
 
-    process(CTXK, lambda: ctx[...].reshape(CTXK, 384), True, nothing)
-    process(BUNDLE, lambda: bundle(0), False, pass_on(1))
-    process(2 * BUNDLE, around(1), False, pass_on(2))
-    process(2 * BUNDLE, around(2), False, pass_last)
+    def stage_own():
+        stage_a(0, 0)
+        stage_b(BUNDLE, x)
+
+    def stage_around(s):
+        def stage():
+            stage_a(0, -s)
+            stage_a(BUNDLE, s)
+
+        return stage
+
+    def stage_last():
+        for i, offset in enumerate((-3, 3, 4)):
+            stage_a(i * BUNDLE, offset)
+        for d in range(1, NX):
+            stage_b((2 + d) * BUNDLE, xp[NX - d])
+
+    pass_on(1, 0)
+    process(CTXK, stage_context, True, ((2, 1, 1), (3, 1, 2)))
+    for copy in bcopies:
+        copy.wait_recv()
+    for copy in lines:
+        copy.start()
+    process(2 * BUNDLE, stage_own, False, ((0, 1, 3), (2, 2, 0), (3, 2, 1)))
+    process(2 * BUNDLE, stage_around(1), False, ((0, 2, 2), (1, 2, 3), (3, 3, 0)))
+    process(2 * BUNDLE, stage_around(2), False, ((0, 3, 1), (1, 3, 2), (2, 3, 3)))
     for j in range(2):
         go_right(4, j).wait_recv()
         go_left(4, j + 2).wait_recv()
-    process(
-        3 * BUNDLE,
-        lambda: jnp.concatenate([bundle(-3), bundle(3), bundle(4)], axis=0),
-        False, nothing, finish,
-    )
+    for copy in lines:
+        copy.wait_recv()
+    process(LAST, stage_last, False, (), finish)
 
     def stat_copy(d):
         return remote(st.at[yp[d]], rst.at[d], ss.at[d], sr.at[d], y=yp[d])
@@ -430,7 +471,7 @@
                 lat[...].astype(F32) + gate_s[...] * (mixed[...] + part)
             ).astype(BF16)
 
-    for copy in xcopies + ccopies + zcopies + ycopies + after + before + hops + kcopies + qcopies:
+    for copy in xcopies + ccopies + zcopies + ycopies + kcopies + qcopies + bcopies + lines:
         copy.wait_send()
 
     @pl.when(mine)
@@ -438,9 +479,14 @@
         for copy in zc:
             copy.wait_send()
 
-    for d in range(3):
+    for d in nearest:
+        eighth_over_y(d).wait_send()
         for i in range(3):
-            across(yp[d], d, i).wait_send()
+            across(d, i).wait_send()
+            if i > 0:
+                over_y(d, i).wait_send()
+        for e in nearest:
+            eighth_over_x(d, e).wait_send()
     for j in range(NX):
         for s in range(1, 4):
             go_right(s, j).wait_send()
@@ -497,14 +543,15 @@
             vmem((NY, 512, 384), BF16), vmem((NY, 256, 256), BF16), vmem((NY, 256, 256), BF16),
             vmem((NX, 3, 512), F32), vmem((NZ, 3, 512), F32), vmem((NY, 4, 512), F32),
             vmem((16, 384), BF16), vmem((NX, 16, 384), BF16), vmem((8, 16, 384), BF16),
-            vmem((ROWS, 384), BF16), vmem((ROWS, 512), BF16),
+            vmem((ROWS, 512), BF16),
             vmem((1, D), F32), vmem((NY, 128), F32),
             vmem((NY, ROWS, 512), BF16),
-            vmem((NZ, NX, ROWS, 384), BF16),
+            vmem((NZ, NX, PIECE_A, 256), BF16), vmem((NX, NZ, PIECE_B, 256), BF16),
             vmem((NY, 384, 512), BF16), vmem((NY, 256, 256), BF16),
             vmem((NY, 2, 256, QN), BF16),
-            vmem((3 * BUNDLE, 256), BF16), vmem((256, 3 * BUNDLE), BF16),
-            vmem((3 * BUNDLE, QN), F32), vmem((3 * BUNDLE, QN), F32),
+            vmem((LAST, 256), BF16), vmem((LAST, 128), BF16),
+            vmem((LAST, 256), BF16), vmem((256, LAST), BF16),
+            vmem((LAST, QN), F32), vmem((LAST, QN), F32),
             vmem((NY, 2, 1, QN), F32), vmem((NY, 2, 1, QN), F32),
             vmem((NY, 2, 128, QN), F32),
             vmem((NY, NY, ROWS, 256), BF16), vmem((NY, NY, ROWS, 256), BF16),
@@ -516,9 +563,12 @@
             dma((NY,)), dma((NY,)),
             dma((NX,)), dma((NX,)),
             dma((NZ,)), dma((2,)),
-            dma((2, 3)), dma((2, 3)),
-            dma((3,)), dma((3,)),
-            dma((3, 3)), dma((3, 3)),
+            dma((NY, 3)), dma((NY, 3)),
+            dma((NY,)), dma((NY,)),
+            dma((NY, NX)), dma((NY, NX)),
+            dma((NY, 3)), dma((NY, 3)),
+            dma((NX,)), dma((NX,)),
+            dma((NZ,)), dma((NZ,)),
             dma((NX,)), dma((NX,)),
             dma((NY,)), dma((NY,)),
             dma((5, NX)), dma((5, NX)),

time: 73.8 us -> 64.1 us (0.87)
  the two profiles are of different devices: /device:TPU:1 before, /device:TPU:2 now
where the time goes in v3:
time: 64.1 us; the launch traced here: 63.8 us
  Pallas kernels  62.1 us (97%)
  local copies, waits for them, and re-layouts  1.77 us (3%)
    pallas_call x1, Pallas kernels, on_device(): pl.pallas_call(kernel, name='whole', out_shape=jax.ShapeDtypeStruct((ROWS...  62.1 us
    unnamed x1, local copies, waits for them, and re-layouts  1.77 us

profile of v3, /device:TPU:2, one launch (start us, length us, event | category | flops | bytes accessed | tf_op | source)
XLA Modules:
  0.0 63.8 jit_solution(13372161704263182305)
XLA Ops:
  0.0 62.1 %whole.1 = bf16[96,2048]{1,0:T(8,128)(2,1)} custom-call(bf16[1,64]{1,0:T(2,128)(2,1)} %bitcast.10, bf16[64,512]{1,0:T(8,128)(2,1)} %sw_h.1, bf16[64,512]{1,0:T(8,128)(2,1)} %cw_h.1, bf16[64,512]{1,0:T(8,128)(2,1)} %gw_h.1, f32[1,2]{1,0:T(1,128)} %bitcast.11, bf16[96,2048]{1,0:T(8,128)(2,1)} %lat_h.1, f32[1,2048]{1,0:T(1,128)} %bitcast.7, f32[1,512]{1,0:T(1,128)} %bitcast.8, ...), custom_call_target="tpu_custom_call" | custom-call | tf_op jit(solution)/shard_map/whole/pallas_call | solution.py:527
  62.1 1.8 %copy.22 = bf16[96,2048]{1,0:T(8,128)(2,1)} copy(bf16[96,2048]{1,0:T(8,128)(2,1)} %whole.1) | data formatting | bytes 786432

commit v4 on v3

--- a/solution.py
+++ b/solution.py
@@ -58,11 +58,17 @@
     cond, sw, cw, gw, bias, lat, gain, qg, lg, rowt, colt, ctxl, ctxr, dq, dl, dr, ow,
     uq, uk, uv, mod_x, mod_z, mod_y, cblk, cx, ctx, qlow, gate_s, bias_s,
     qa, zka, zkb, wq_t, wv_t, q_t, lows, ropes, kn, vt, sa, sb, m_s, l_s, acc, ob, rb, st, rst, mixed,
-    in_sem, own_sem, xs, xr, zs, zr, ys, yr, cxs, cxr, czs, czr, ws, wr, hs, hr, es, er, fs, fr,
-    ks, kr, bs, br, js, jr, qs, qr, rs, rr, ls, lr, os, orr, ss, sr,
+    in_sem, own_sem, snd, rcv,
 ):
     z, x, y, c = (lax.axis_index(n) for n in ("z", "x", "y", "c"))
     sp = z * NX + x
+
+    def drain(ref, i):
+        remote(ref, ref, snd.at[i], rcv.at[0], c=1 - c).wait_send()
+
+    def landed(ref, i):
+        remote(ref, ref, snd.at[0], rcv.at[i], c=1 - c).wait_recv()
+
     fetches = [
         pltpu.make_async_copy(h, v, in_sem.at[i])
         for i, (h, v) in enumerate((
@@ -75,7 +81,7 @@
         pltpu.make_async_copy(h, v.at[y], own_sem.at[i])
         for i, (h, v) in enumerate(((uq_h, uq), (uk_h, uk), (uv_h, uv)))
     ]
-    for copy in fetches[:8] + owns + fetches[8:]:
+    for copy in fetches[:7] + owns:
         copy.start()
     xp = [lax.rem(x + d, NX) for d in range(NX)]
     yp = [lax.rem(y + d, NY) for d in range(NY)]
@@ -96,17 +102,19 @@
     v = cond[...].astype(F32)
     activated = (v / (1.0 + jnp.exp(-v))).astype(BF16)
     mod_x[x] = jnp.concatenate([dot(activated, w[...]) for w in (sw, cw, gw)], axis=0)
+    pl.semaphore_wait(barrier, len(peers))
+    xcopies = [
+        remote(mod_x.at[x], mod_x.at[x], snd.at[0], rcv.at[0], x=xp[d]) for d in range(1, NX)
+    ]
+    for copy in xcopies:
+        copy.start()
+    for copy in fetches[7:]:
+        copy.start()
     for copy in owns:
         copy.wait()
-    pl.semaphore_wait(barrier, len(peers))
-    xcopies = [
-        remote(mod_x.at[x], mod_x.at[x], xs.at[d], xr.at[d], x=xp[d]) for d in range(1, NX)
-    ]
-    for copy in xcopies:
-        copy.start()
     cblk[...] = jnp.concatenate([ctxl[...], ctxr[...], jnp.zeros((16, 64), BF16)], axis=1)
     cx[x] = cblk[...]
-    ccopies = [remote(cblk, cx.at[x], cxs.at[d], cxr.at[d], x=xp[d]) for d in range(1, NX)]
+    ccopies = [remote(cblk, cx.at[x], snd.at[1], rcv.at[1], x=xp[d]) for d in range(1, NX)]
     for copy in ccopies:
         copy.start()
 
@@ -118,32 +126,30 @@
         return uq.at[slot, pl.ds(pl.multiple_of(c * 256 + x * 64, 64), 64)]
 
     def over_y(d, i):
-        return remote(half(ups[i], y), half(ups[i], y), ws.at[d, i], wr.at[d, i], y=yp[d])
+        return remote(half(ups[i], y), half(ups[i], y), snd.at[5 + i], rcv.at[6 + i], y=yp[d])
 
     def eighth_over_y(d):
-        return remote(eighth(y), eighth(y), hs.at[d], hr.at[d], y=yp[d])
+        return remote(eighth(y), eighth(y), snd.at[5], rcv.at[6], y=yp[d])
 
     def eighth_over_x(d, e):
         slot = yp[NY - d]
-        return remote(eighth(slot), eighth(slot), es.at[d, e], er.at[d, e], x=xp[e])
+        return remote(eighth(slot), eighth(slot), snd.at[8], rcv.at[9], x=xp[e])
 
     def across(d, i):
         slot = yp[NY - d]
-        return remote(half(ups[i], slot), half(ups[i], slot), fs.at[d, i], fr.at[d, i], c=1 - c)
+        return remote(half(ups[i], slot), half(ups[i], slot), snd.at[9 + i], rcv.at[10 + i], c=1 - c)
 
     ups = (uq, uk, uv)
     nearest = (1, 3, 2)
     for d in nearest:
         eighth_over_y(d).start()
-    for i in (1, 2):
-        for d in nearest:
-            over_y(d, i).start()
-
-    for copy in xcopies:
-        copy.wait_recv()
+    for d in nearest:
+        over_y(d, 1).start()
+
+    landed(mod_x.at[0:3], 0)
     mod_z[z] = mod_x[0] + mod_x[1] + mod_x[2] + mod_x[3]
     zcopies = [
-        remote(mod_z.at[z], mod_z.at[z], zs.at[d], zr.at[d], z=zp[d]) for d in range(1, NZ)
+        remote(mod_z.at[z], mod_z.at[z], snd.at[2], rcv.at[2], z=zp[d]) for d in range(1, NZ)
     ]
     for copy in zcopies:
         copy.start()
@@ -167,13 +173,12 @@
     m_s[...] = jnp.full(m_s.shape, NEG, F32)
     l_s[...] = jnp.zeros(l_s.shape, F32)
     acc[...] = jnp.zeros(acc.shape, F32)
-    for copy in ccopies:
-        copy.wait_recv()
+    landed(cx.at[0:3], 1)
     mine = z // 2 == y
     zc = [
         remote(
-            cx, ctx.at[pl.ds(pl.multiple_of((z % 2) * NX, NX), NX)], czs.at[d],
-            czr.at[z % 2], z=zp[d],
+            cx, ctx.at[pl.ds(pl.multiple_of((z % 2) * NX, NX), NX)], snd.at[4],
+            rcv.at[4 + z % 2], z=zp[d],
         )
         for d in range(1, NZ)
     ]
@@ -184,30 +189,32 @@
         for copy in zc:
             copy.start()
 
-    for d in nearest:
-        eighth_over_y(d).wait_recv()
+    landed(uq.at[0, 0:192], 6)
+    for d in nearest:
         for e in nearest:
             eighth_over_x(d, e).start()
 
-    for copy in zcopies:
-        copy.wait_recv()
+    landed(mod_z.at[0:7], 2)
     total = mod_z[0]
     for k in range(1, NZ):
         total = total + mod_z[k]
     bias_row = jnp.concatenate([bias[...], jnp.zeros((1, 510), F32)], axis=1)
     mod_y[y] = jnp.concatenate([total, bias_row], axis=0)
     ycopies = [
-        remote(mod_y.at[y], mod_y.at[y], ys.at[d], yr.at[d], y=yp[d]) for d in range(1, NY)
+        remote(mod_y.at[y], mod_y.at[y], snd.at[3], rcv.at[3], y=yp[d]) for d in range(1, NY)
     ]
     for copy in ycopies:
         copy.start()
-    for i in (1, 2):
-        for d in nearest:
-            over_y(d, i).wait_recv()
-            across(d, i).start()
-
-    for copy in ycopies:
-        copy.wait_recv()
+    for d in nearest:
+        over_y(d, 2).start()
+    landed(uk.at[0:3, 0:128], 7)
+    for d in nearest:
+        across(d, 1).start()
+
+    landed(mod_y.at[0:3], 3)
+    landed(uq.at[0:3, 0:192], 9)
+    for d in nearest:
+        across(d, 0).start()
     shift = jnp.concatenate([mod_y[k, 0:1] for k in range(NY)], axis=1)
     scale = jnp.concatenate([mod_y[k, 1:2] for k in range(NY)], axis=1)
     gate_s[...] = jnp.concatenate([mod_y[k, 2:3] for k in range(NY)], axis=1)
@@ -220,7 +227,7 @@
         return a * lax.rsqrt(jnp.mean(a * a, axis=-1, keepdims=True) + EPS) * g
 
     qlow[...] = rms(dot(normed, dq[...]), qg[...]).astype(BF16)
-    qcopies = [remote(qlow, qa.at[y], qs.at[d], qr.at[d], y=yp[d]) for d in range(1, NY)]
+    qcopies = [remote(qlow, qa.at[y], snd.at[12], rcv.at[13], y=yp[d]) for d in range(1, NY)]
     for copy in qcopies:
         copy.start()
     low = rms(dot(normed, dl[...]), lg[...]).astype(BF16)
@@ -245,51 +252,61 @@
     def piece(offset, j):
         return zka.at[slot_of(offset), lax.rem(x - piece_order(j) + NX, NX)]
 
+    def turn(s, j):
+        return rcv.at[29 if s == 4 else 13 + 4 * s + j]
+
     def go_right(s, j):
-        return remote(piece(1 - s, j), piece(1 - s, j), rs.at[s, j], rr.at[s, j], z=right)
+        return remote(piece(1 - s, j), piece(1 - s, j), snd.at[14], turn(s, j), z=right)
 
     def go_left(s, j):
-        return remote(piece(s - 1, j), piece(s - 1, j), ls.at[s, j], lr.at[s, j], z=left)
+        return remote(piece(s - 1, j), piece(s - 1, j), snd.at[14], turn(s, j), z=left)
 
     kcopies = [
-        remote(zka.at[z, x], zka.at[z, x], ks.at[d], kr.at[d], x=xp[d]) for d in range(1, NX)
-    ]
-    bcopies = [
-        remote(zkb.at[x, z], zkb.at[x, z], bs.at[d], br.at[d], z=zp[d]) for d in range(1, NZ)
-    ]
-    lines = [remote(zkb.at[x], zkb.at[x], js.at[d], jr.at[d], x=xp[d]) for d in range(1, NX)]
+        remote(zka.at[z, x], zka.at[z, x], snd.at[13], rcv.at[13 + d], x=xp[d]) for d in range(1, NX)
+    ]
+    def along_z(origin, d, to):
+        held = zkb.at[x, slot_of(origin)]
+        group = 30 if d in (2, 6) else 31 if d in (1, 7) else 32
+        return remote(held, held, snd.at[15], rcv.at[group], z=to)
+
+    def along_x(o, d):
+        held = zkb.at[x, slot_of(-o)]
+        return remote(held, held, snd.at[16], rcv.at[33], x=xp[d])
+
     for copy in kcopies:
         copy.start()
     go_right(1, 0).start()
     go_left(1, 0).start()
-    for copy in bcopies:
-        copy.start()
+    for d in (1, 7, 2, 6):
+        along_z(0, d, zp[d]).start()
+    for d in nearest:
+        along_x(0, d).start()
     qa[y] = qlow[...]
 
-    for d in nearest:
-        for e in nearest:
-            eighth_over_x(d, e).wait_recv()
-        across(d, 0).start()
+    landed(uv.at[0:3, 0:128], 8)
+    for d in nearest:
+        across(d, 2).start()
+    landed(uq.at[0:3, 0:256], 10)
+    for d in nearest:
+        slot = yp[NY - d]
+        wq_t[slot] = uq[slot].T
     for j, d in ((1, 1), (2, 3), (3, 2)):
         kcopies[d - 1].wait_recv()
         go_right(1, j).start()
         go_left(1, j).start()
-    for d in nearest:
-        for i in (1, 2, 0):
-            across(d, i).wait_recv()
+    landed(uk.at[0:3, 0:128], 11)
+    landed(uv.at[0:3, 0:128], 12)
+    for d in nearest:
         slot = yp[NY - d]
-        wq_t[slot] = uq[slot].T
         wv_t[slot] = uv[slot].T
     for k in range(2):
         @pl.when(z != 2 * y + k)
         def _():
-            remote(cx, ctx.at[pl.ds(k * NX, NX)], czs.at[0], czr.at[k], z=zp[1]).wait_recv()
-
-    for copy in qcopies:
-        copy.wait_recv()
-
-    @pl.loop(0, NY)
-    def _(k):
+            landed(ctx.at[pl.ds(k * NX, NX)], 4 + k)
+
+    landed(qa.at[0:3], 13)
+
+    for k in range(NY):
         qt = dot_nt(wq_t[k], qa[...].reshape(QN, 512))
         for h in range(2):
             b = 192 * h
@@ -312,48 +329,50 @@
         return p.astype(BF16), shrink
 
     def pass_on(s, j):
-        go_right(s, j).wait_recv()
-        go_left(s, j).wait_recv()
+        landed(zka.at[0, 0:2], 13 + 4 * s + j)
         if s < 3 or j < 2:
             go_right(s + 1, j).start()
         if s < 3 or j >= 2:
             go_left(s + 1, j).start()
 
-    def process(n, stage, biased, passes, finish=None):
-        def project(k):
-            return dot(lows[0:n], uk[k]).astype(BF16), dot_nt(wv_t[k], lows[0:n]).astype(BF16)
-
-        def score(nope, h, k):
-            key = jnp.concatenate([nope[:, 128 * h : 128 * h + 128], ropes[0:n]], axis=1)
-            return dot(key, q_t[k, h])
-
+    def project(n, k):
+        return dot(lows[0:n], uk[k]).astype(BF16), dot_nt(wv_t[k], lows[0:n]).astype(BF16)
+
+    def score(nope, n, k, h):
+        key = jnp.concatenate([nope[:, 128 * h : 128 * h + 128], ropes[0:n]], axis=1)
+        return dot(key, q_t[k, h])
+
+    def weigh(s_ref, n, k, h, biased):
+        p, shrink = softmax(s_ref, n, k, h, biased)
+        acc[k, h] = acc[k, h] * shrink + dot(vt[128 * h : 128 * h + 128, 0:n], p)
+
+    def attend(n, stage, biased, passes, finish):
         def step(k, final):
             for at, s, j in passes:
                 if final and at == NY - 1:
                     pass_on(s, j)
                 elif not final and at < NY - 1:
                     pl.when(k == at)(lambda s=s, j=j: pass_on(s, j))
-            now = kn[0:n]
-            sb[0:n] = score(now, 1, k)
+            sb[0:n] = score(kn[0:n], n, k, 1)
             if not final:
-                nope, val = project(k + 1)
-            p, shrink = softmax(sa, n, k, 0, biased)
-            acc[k, 0] = acc[k, 0] * shrink + dot(vt[0:128, 0:n], p)
-            if not final:
-                sa[0:n] = score(nope, 0, k + 1)
-            p, shrink = softmax(sb, n, k, 1, biased)
-            acc[k, 1] = acc[k, 1] * shrink + dot(vt[128:256, 0:n], p)
+                nope, val = project(n, k + 1)
+            weigh(sa, n, k, 0, biased)
+            if final:
+                finish(k, 0)
+            else:
+                sa[0:n] = score(nope, n, k + 1, 0)
+            weigh(sb, n, k, 1, biased)
             if not final:
                 kn[0:n] = nope
                 vt[:, 0:n] = val
-            if finish is not None:
-                finish(k)
+                finish(k, 0)
+            finish(k, 1)
 
         stage()
-        nope, val = project(0)
+        nope, val = project(n, 0)
         kn[0:n] = nope
         vt[:, 0:n] = val
-        sa[0:n] = score(nope, 0, 0)
+        sa[0:n] = score(nope, n, 0, 0)
 
         @pl.loop(0, NY - 1)
         def _(k):
@@ -384,33 +403,33 @@
             ropes[first : first + 16] = tile
             ropes[first + 16 : first + 32] = lane_pair(tile)
 
-    def out_copy(k, d):
-        return remote(ob.at[k, yp[d]], rb.at[d, k], os.at[d, k], orr.at[d, k], y=yp[d])
-
-    def finish(k):
-        both = []
-        for h in range(2):
-            total = l_s[k, h]
-            both.append((acc[k, h] / total).T)
-            row = m_s[k, h] + jnp.log2(total)
-            for j in range(NY):
-                st[j, k, h : h + 1] = jnp.concatenate(
-                    [row[:, ROWS * j : ROWS * j + ROWS], jnp.zeros((1, 32), F32)], axis=1
-                )
-        ob[k] = jnp.concatenate(both, axis=1).astype(BF16).reshape(NY, ROWS, 256)
+    def out_copy(k, h, d):
+        return remote(ob.at[k, h, yp[d]], rb.at[k, d - 1, h], snd.at[17], rcv.at[34 + k], y=yp[d])
+
+    def stat_copy(k, d):
+        return remote(st.at[yp[d], k], rst.at[k, d - 1], snd.at[18], rcv.at[38 + k], y=yp[d])
+
+    def finish(k, h):
+        total = l_s[k, h]
+        row = m_s[k, h] + jnp.log2(total)
+        for j in range(NY):
+            st[j, k, h : h + 1] = jnp.concatenate(
+                [row[:, ROWS * j : ROWS * j + ROWS], jnp.zeros((1, 32), F32)], axis=1
+            )
+        ob[k, h] = (acc[k, h] / total).T.astype(BF16).reshape(NY, ROWS, 128)
         for d in range(1, NY):
-            out_copy(k, d).start()
-
-    def stage_own():
-        stage_a(0, 0)
-        stage_b(BUNDLE, x)
-
-    def stage_around(s):
-        def stage():
-            stage_a(0, -s)
-            stage_a(BUNDLE, s)
-
-        return stage
+            if h == 1:
+                stat_copy(k, d).start()
+            out_copy(k, h, d).start()
+
+    def stage_first():
+        stage_b(0, x)
+        stage_a(BUNDLE, -1)
+        stage_a(2 * BUNDLE, 1)
+
+    def stage_second():
+        stage_a(0, -2)
+        stage_a(BUNDLE, 2)
 
     def stage_last():
         for i, offset in enumerate((-3, 3, 4)):
@@ -418,48 +437,55 @@
         for d in range(1, NX):
             stage_b((2 + d) * BUNDLE, xp[NX - d])
 
-    pass_on(1, 0)
-    process(CTXK, stage_context, True, ((2, 1, 1), (3, 1, 2)))
-    for copy in bcopies:
-        copy.wait_recv()
-    for copy in lines:
-        copy.start()
-    process(2 * BUNDLE, stage_own, False, ((0, 1, 3), (2, 2, 0), (3, 2, 1)))
-    process(2 * BUNDLE, stage_around(1), False, ((0, 2, 2), (1, 2, 3), (3, 3, 0)))
-    process(2 * BUNDLE, stage_around(2), False, ((0, 3, 1), (1, 3, 2), (2, 3, 3)))
-    for j in range(2):
-        go_right(4, j).wait_recv()
-        go_left(4, j + 2).wait_recv()
-    for copy in lines:
-        copy.wait_recv()
-    process(LAST, stage_last, False, (), finish)
-
-    def stat_copy(d):
-        return remote(st.at[yp[d]], rst.at[d], ss.at[d], sr.at[d], y=yp[d])
-
-    for d in range(1, NY):
-        stat_copy(d).start()
-    for d in range(1, NY):
-        stat_copy(d).wait_recv()
-    stats = [st[y]] + [rst[d] for d in range(1, NY)]
-    top = jnp.maximum(jnp.maximum(stats[0], stats[1]), jnp.maximum(stats[2], stats[3]))
-    raised = [jnp.exp2(s - top) for s in stats]
-    whole = raised[0] + raised[1] + raised[2] + raised[3]
-    fill = jnp.zeros((120, 128), F32)
-    shares = [
-        jnp.concatenate([(r / whole).reshape(8, 128), fill], axis=0).T[:ROWS] for r in raised
-    ]
+    def nothing(*_):
+        pass
+
+    landed(zkb.at[0, 0:2], 30)
+    along_z(-2, 3, right).start()
+    along_z(2, 5, left).start()
+
+    @pl.when(z % 2 == 0)
+    def _():
+        along_z(-2, 4, zp[2]).start()
+
+    @pl.when(z % 2 == 1)
+    def _():
+        along_z(2, 4, zp[6]).start()
+
+    landed(zkb.at[0, 0:2], 31)
+    for o in (1, 7, 2, 6):
+        for d in nearest:
+            along_x(o, d).start()
+    attend(CTXK, stage_context, True, ((2, 1, 0), (3, 1, 1)), nothing)
+    attend(BUNDLE, lambda: stage_a(0, 0), False, ((1, 1, 2), (3, 1, 3)), nothing)
+    landed(zkb.at[0, 0:3], 32)
+    for o in (3, 5, 4):
+        for d in nearest:
+            along_x(o, d).start()
+    attend(
+        3 * BUNDLE, stage_first, False,
+        ((0, 2, 0), (1, 2, 1), (1, 2, 2), (2, 2, 3), (2, 3, 0), (3, 3, 1), (3, 3, 2)), nothing,
+    )
+    attend(2 * BUNDLE, stage_second, False, ((0, 3, 3),), nothing)
+    landed(zka.at[0], 29)
+    landed(zkb.at[0:3], 33)
+    attend(LAST, stage_last, False, (), finish)
+
     fetches[16].wait()
+    fill = jnp.zeros((6, 128), F32)
     for k in range(NY):
-        for d in range(1, NY):
-            out_copy(k, d).wait_recv()
-        pieces = [ob[k, y]] + [rb[d, k] for d in range(1, NY)]
+        landed(rst.at[k], 38 + k)
+        landed(rb.at[k], 34 + k)
+        stats = [st[y, k]] + [rst[k, d - 1] for d in range(1, NY)]
+        top = jnp.maximum(jnp.maximum(stats[0], stats[1]), jnp.maximum(stats[2], stats[3]))
+        raised = [jnp.exp2(v - top) for v in stats]
+        whole = raised[0] + raised[1] + raised[2] + raised[3]
+        shares = [jnp.concatenate([r / whole, fill], axis=0).T[:ROWS] for r in raised]
         both = []
         for h in range(2):
-            head = 2 * k + h
+            pieces = [ob[k, h, y]] + [rb[k, d - 1, h] for d in range(1, NY)]
             both.append(sum(
-                p[:, 128 * h : 128 * h + 128].astype(F32) * share[:, head : head + 1]
-                for p, share in zip(pieces, shares)
+                p.astype(F32) * share[:, h : h + 1] for p, share in zip(pieces, shares)
             ))
         part = dot(jnp.concatenate(both, axis=1).astype(BF16), ow[256 * k : 256 * k + 256])
         if k == 0:
@@ -471,34 +497,18 @@
                 lat[...].astype(F32) + gate_s[...] * (mixed[...] + part)
             ).astype(BF16)
 
-    for copy in xcopies + ccopies + zcopies + ycopies + kcopies + qcopies + bcopies + lines:
-        copy.wait_send()
+    for ref, i in (
+        (mod_x.at[0:3], 0), (cx.at[0:3], 1), (mod_z.at[0:7], 2), (mod_y.at[0:3], 3),
+        (uq.at[0, 0:192], 5), (uk.at[0:3, 0:128], 6), (uv.at[0:3, 0:128], 7),
+        (uq.at[0:3, 0:192], 8), (uq.at[0:3, 0:256], 9), (uk.at[0:3, 0:128], 10),
+        (uv.at[0:3, 0:128], 11), (qa.at[0:3], 12), (zka.at[0, 0:3], 13), (zka.at[0:7], 14),
+        (zkb.at[0, 0:7], 15), (zkb.at[0:3], 16), (ob.at[:, :, 0:3], 17), (st.at[0:3], 18),
+    ):
+        drain(ref, i)
 
     @pl.when(mine)
     def _():
-        for copy in zc:
-            copy.wait_send()
-
-    for d in nearest:
-        eighth_over_y(d).wait_send()
-        for i in range(3):
-            across(d, i).wait_send()
-            if i > 0:
-                over_y(d, i).wait_send()
-        for e in nearest:
-            eighth_over_x(d, e).wait_send()
-    for j in range(NX):
-        for s in range(1, 4):
-            go_right(s, j).wait_send()
-            go_left(s, j).wait_send()
-        if j < 2:
-            go_right(4, j).wait_send()
-        else:
-            go_left(4, j).wait_send()
-    for d in range(1, NY):
-        stat_copy(d).wait_send()
-        for k in range(NY):
-            out_copy(k, d).wait_send()
+        drain(uq.at[0, 0:448], 4)
 
 
 def rope_constants():
@@ -554,27 +564,10 @@
             vmem((LAST, QN), F32), vmem((LAST, QN), F32),
             vmem((NY, 2, 1, QN), F32), vmem((NY, 2, 1, QN), F32),
             vmem((NY, 2, 128, QN), F32),
-            vmem((NY, NY, ROWS, 256), BF16), vmem((NY, NY, ROWS, 256), BF16),
-            vmem((NY, NY, 2, 128), F32), vmem((NY, NY, 2, 128), F32),
+            vmem((NY, 2, NY, ROWS, 128), BF16), vmem((NY, NY - 1, 2, ROWS, 128), BF16),
+            vmem((NY, NY, 2, 128), F32), vmem((NY, NY - 1, 2, 128), F32),
             vmem((ROWS, D), F32),
-            dma((17,)), dma((3,)),
-            dma((NX,)), dma((NX,)),
-            dma((NZ,)), dma((NZ,)),
-            dma((NY,)), dma((NY,)),
-            dma((NX,)), dma((NX,)),
-            dma((NZ,)), dma((2,)),
-            dma((NY, 3)), dma((NY, 3)),
-            dma((NY,)), dma((NY,)),
-            dma((NY, NX)), dma((NY, NX)),
-            dma((NY, 3)), dma((NY, 3)),
-            dma((NX,)), dma((NX,)),
-            dma((NZ,)), dma((NZ,)),
-            dma((NX,)), dma((NX,)),
-            dma((NY,)), dma((NY,)),
-            dma((5, NX)), dma((5, NX)),
-            dma((5, NX)), dma((5, NX)),
-            dma((NY, NY)), dma((NY, NY)),
-            dma((NY,)), dma((NY,)),
+            dma((17,)), dma((3,)), dma((19,)), dma((42,)),
         ],
         compiler_params=pltpu.CompilerParams(
             collective_id=0, has_side_effects=True, vmem_limit_bytes=60 * 1024 * 1024

time: 64.1 us -> 61.3 us (0.956)
  Pallas kernels: 62.1 us -> 58.8 us
    pallas_call x1, Pallas kernels: 62.1 us -> 58.8 us  [on_device(): pl.pallas_call(kernel, name='whole', out_shape=jax.ShapeDtypeStruct((ROWS...]
where the time goes in v4:
time: 61.3 us; the launch traced here: 60.6 us
  Pallas kernels  58.8 us (96%)
  local copies, waits for them, and re-layouts  1.77 us (3%)
    pallas_call x1, Pallas kernels, on_device(): pl.pallas_call(kernel, name='whole', out_shape=jax.ShapeDtypeStruct((ROWS...  58.8 us
    unnamed x1, local copies, waits for them, and re-layouts  1.77 us

profile of v4, /device:TPU:2, one launch (start us, length us, event | category | flops | bytes accessed | tf_op | source)
XLA Modules:
  0.0 60.6 jit_solution(1861674541654447509)
XLA Ops:
  0.0 58.8 %whole.1 = bf16[96,2048]{1,0:T(8,128)(2,1)} custom-call(bf16[1,64]{1,0:T(2,128)(2,1)} %bitcast.10, bf16[64,512]{1,0:T(8,128)(2,1)} %sw_h.1, bf16[64,512]{1,0:T(8,128)(2,1)} %cw_h.1, bf16[64,512]{1,0:T(8,128)(2,1)} %gw_h.1, f32[1,2]{1,0:T(1,128)} %bitcast.11, bf16[96,2048]{1,0:T(8,128)(2,1)} %lat_h.1, f32[1,2048]{1,0:T(1,128)} %bitcast.7, f32[1,512]{1,0:T(1,128)} %bitcast.8, ...), custom_call_target="tpu_custom_call" | custom-call | tf_op jit(solution)/shard_map/whole/pallas_call | solution.py:537
  58.8 1.8 %copy.22 = bf16[96,2048]{1,0:T(8,128)(2,1)} copy(bf16[96,2048]{1,0:T(8,128)(2,1)} %whole.1) | data formatting | bytes 786432

commit v5 on v4

--- a/solution.py
+++ b/solution.py
@@ -87,6 +87,7 @@
     yp = [lax.rem(y + d, NY) for d in range(NY)]
     zp = [lax.rem(z + d, NZ) for d in range(NZ)]
     right, left = zp[1], zp[NZ - 1]
+    farthest = (2, 1, 3)
     peers = (
         [{"x": xp[d]} for d in range(1, NX)]
         + [{"y": yp[d]} for d in range(1, NY)]
@@ -104,7 +105,7 @@
     mod_x[x] = jnp.concatenate([dot(activated, w[...]) for w in (sw, cw, gw)], axis=0)
     pl.semaphore_wait(barrier, len(peers))
     xcopies = [
-        remote(mod_x.at[x], mod_x.at[x], snd.at[0], rcv.at[0], x=xp[d]) for d in range(1, NX)
+        remote(mod_x.at[x], mod_x.at[x], snd.at[0], rcv.at[0], x=xp[d]) for d in farthest
     ]
     for copy in xcopies:
         copy.start()
@@ -114,7 +115,7 @@
         copy.wait()
     cblk[...] = jnp.concatenate([ctxl[...], ctxr[...], jnp.zeros((16, 64), BF16)], axis=1)
     cx[x] = cblk[...]
-    ccopies = [remote(cblk, cx.at[x], snd.at[1], rcv.at[1], x=xp[d]) for d in range(1, NX)]
+    ccopies = [remote(cblk, cx.at[x], snd.at[1], rcv.at[1], x=xp[d]) for d in farthest]
     for copy in ccopies:
         copy.start()
 
@@ -140,16 +141,16 @@
         return remote(half(ups[i], slot), half(ups[i], slot), snd.at[9 + i], rcv.at[10 + i], c=1 - c)
 
     ups = (uq, uk, uv)
-    nearest = (1, 3, 2)
-    for d in nearest:
+    for d in farthest:
         eighth_over_y(d).start()
-    for d in nearest:
+    for d in farthest:
         over_y(d, 1).start()
 
     landed(mod_x.at[0:3], 0)
     mod_z[z] = mod_x[0] + mod_x[1] + mod_x[2] + mod_x[3]
     zcopies = [
-        remote(mod_z.at[z], mod_z.at[z], snd.at[2], rcv.at[2], z=zp[d]) for d in range(1, NZ)
+        remote(mod_z.at[z], mod_z.at[z], snd.at[2], rcv.at[2], z=zp[d])
+        for d in (4, 3, 5, 2, 6, 1, 7)
     ]
     for copy in zcopies:
         copy.start()
@@ -190,8 +191,8 @@
             copy.start()
 
     landed(uq.at[0, 0:192], 6)
-    for d in nearest:
-        for e in nearest:
+    for d in farthest:
+        for e in farthest:
             eighth_over_x(d, e).start()
 
     landed(mod_z.at[0:7], 2)
@@ -201,19 +202,19 @@
     bias_row = jnp.concatenate([bias[...], jnp.zeros((1, 510), F32)], axis=1)
     mod_y[y] = jnp.concatenate([total, bias_row], axis=0)
     ycopies = [
-        remote(mod_y.at[y], mod_y.at[y], snd.at[3], rcv.at[3], y=yp[d]) for d in range(1, NY)
+        remote(mod_y.at[y], mod_y.at[y], snd.at[3], rcv.at[3], y=yp[d]) for d in farthest
     ]
     for copy in ycopies:
         copy.start()
-    for d in nearest:
+    for d in farthest:
         over_y(d, 2).start()
     landed(uk.at[0:3, 0:128], 7)
-    for d in nearest:
+    for d in farthest:
         across(d, 1).start()
 
     landed(mod_y.at[0:3], 3)
     landed(uq.at[0:3, 0:192], 9)
-    for d in nearest:
+    for d in farthest:
         across(d, 0).start()
     shift = jnp.concatenate([mod_y[k, 0:1] for k in range(NY)], axis=1)
     scale = jnp.concatenate([mod_y[k, 1:2] for k in range(NY)], axis=1)
@@ -227,7 +228,7 @@
         return a * lax.rsqrt(jnp.mean(a * a, axis=-1, keepdims=True) + EPS) * g
 
     qlow[...] = rms(dot(normed, dq[...]), qg[...]).astype(BF16)
-    qcopies = [remote(qlow, qa.at[y], snd.at[12], rcv.at[13], y=yp[d]) for d in range(1, NY)]
+    qcopies = [remote(qlow, qa.at[y], snd.at[12], rcv.at[13], y=yp[d]) for d in farthest]
     for copy in qcopies:
         copy.start()
     low = rms(dot(normed, dl[...]), lg[...]).astype(BF16)
@@ -253,13 +254,26 @@
         return zka.at[slot_of(offset), lax.rem(x - piece_order(j) + NX, NX)]
 
     def turn(s, j):
-        return rcv.at[29 if s == 4 else 13 + 4 * s + j]
+        return rcv.at[13 + 4 * s + j]
 
     def go_right(s, j):
         return remote(piece(1 - s, j), piece(1 - s, j), snd.at[14], turn(s, j), z=right)
 
     def go_left(s, j):
         return remote(piece(s - 1, j), piece(s - 1, j), snd.at[14], turn(s, j), z=left)
+
+    def two_right(j):
+        return remote(piece(-2, j), piece(-2, j), snd.at[14], rcv.at[29], z=zp[2])
+
+    def two_left(j):
+        return remote(piece(2, j), piece(2, j), snd.at[14], rcv.at[29], z=zp[NZ - 2])
+
+    def pass_on(s, j):
+        landed(zka.at[0, 0:2], 13 + 4 * s + j)
+        go_right(s + 1, j).start()
+        go_left(s + 1, j).start()
+        if s == 2:
+            (two_right if j < 2 else two_left)(j).start()
 
     kcopies = [
         remote(zka.at[z, x], zka.at[z, x], snd.at[13], rcv.at[13 + d], x=xp[d]) for d in range(1, NX)
@@ -273,30 +287,31 @@
         held = zkb.at[x, slot_of(-o)]
         return remote(held, held, snd.at[16], rcv.at[33], x=xp[d])
 
-    for copy in kcopies:
-        copy.start()
+    for d in farthest:
+        kcopies[d - 1].start()
     go_right(1, 0).start()
     go_left(1, 0).start()
-    for d in (1, 7, 2, 6):
+    for d in (2, 6, 1, 7):
         along_z(0, d, zp[d]).start()
-    for d in nearest:
+    for d in farthest:
         along_x(0, d).start()
     qa[y] = qlow[...]
 
     landed(uv.at[0:3, 0:128], 8)
-    for d in nearest:
+    for d in farthest:
         across(d, 2).start()
     landed(uq.at[0:3, 0:256], 10)
-    for d in nearest:
+    for d in farthest:
         slot = yp[NY - d]
         wq_t[slot] = uq[slot].T
+    pass_on(1, 0)
     for j, d in ((1, 1), (2, 3), (3, 2)):
         kcopies[d - 1].wait_recv()
         go_right(1, j).start()
         go_left(1, j).start()
     landed(uk.at[0:3, 0:128], 11)
     landed(uv.at[0:3, 0:128], 12)
-    for d in nearest:
+    for d in farthest:
         slot = yp[NY - d]
         wv_t[slot] = uv[slot].T
     for k in range(2):
@@ -318,22 +333,20 @@
             ).astype(BF16)
 
     def softmax(s_ref, n, k, h, biased):
-        top = jnp.max(s_ref[0:n], axis=0, keepdims=True) * SCALE2
-        lift = bias_s[pl.ds(k, 1), h : h + 1] * LOG2E if biased else None
-        m_old = m_s[k, h]
-        m_new = jnp.maximum(m_old, top + lift if biased else top)
-        p = jnp.exp2(s_ref[0:n] * SCALE2 - (m_new - lift if biased else m_new))
+        parts = [(biased, n, 0.0)]
+        if biased:
+            parts = [(0, biased, bias_s[pl.ds(k, 1), h : h + 1] * LOG2E)] + parts
+        m_old = m_new = m_s[k, h]
+        for a, b, lift in parts:
+            top = jnp.max(s_ref[a:b], axis=0, keepdims=True) * SCALE2
+            m_new = jnp.maximum(m_new, top + lift)
+        p = jnp.concatenate(
+            [jnp.exp2(s_ref[a:b] * SCALE2 - (m_new - lift)) for a, b, lift in parts], axis=0
+        )
         shrink = jnp.exp2(m_old - m_new)
         l_s[k, h] = l_s[k, h] * shrink + jnp.sum(p, axis=0, keepdims=True)
         m_s[k, h] = m_new
         return p.astype(BF16), shrink
-
-    def pass_on(s, j):
-        landed(zka.at[0, 0:2], 13 + 4 * s + j)
-        if s < 3 or j < 2:
-            go_right(s + 1, j).start()
-        if s < 3 or j >= 2:
-            go_left(s + 1, j).start()
 
     def project(n, k):
         return dot(lows[0:n], uk[k]).astype(BF16), dot_nt(wv_t[k], lows[0:n]).astype(BF16)
@@ -380,11 +393,6 @@
 
         step(NY - 1, True)
 
-    def stage_context():
-        both = ctx[...].reshape(CTXK, 384)
-        lows[0:CTXK] = both[:, :256]
-        ropes[0:CTXK] = both[:, 256:]
-
     def stage_a(at, offset):
         slot = slot_of(offset)
         lows[at : at + BUNDLE] = zka[slot, :, :ROWS_A].reshape(BUNDLE, 256)
@@ -417,10 +425,16 @@
                 [row[:, ROWS * j : ROWS * j + ROWS], jnp.zeros((1, 32), F32)], axis=1
             )
         ob[k, h] = (acc[k, h] / total).T.astype(BF16).reshape(NY, ROWS, 128)
-        for d in range(1, NY):
+        for d in farthest:
             if h == 1:
                 stat_copy(k, d).start()
             out_copy(k, h, d).start()
+
+    def stage_own():
+        both = ctx[...].reshape(CTXK, 384)
+        lows[0:CTXK] = both[:, :256]
+        ropes[0:CTXK] = both[:, 256:]
+        stage_a(CTXK, 0)
 
     def stage_first():
         stage_b(0, x)
@@ -454,22 +468,25 @@
 
     landed(zkb.at[0, 0:2], 31)
     for o in (1, 7, 2, 6):
-        for d in nearest:
+        for d in farthest:
             along_x(o, d).start()
-    attend(CTXK, stage_context, True, ((2, 1, 0), (3, 1, 1)), nothing)
-    attend(BUNDLE, lambda: stage_a(0, 0), False, ((1, 1, 2), (3, 1, 3)), nothing)
+    attend(CTXK + BUNDLE, stage_own, CTXK, ((1, 2, 0), (3, 1, 1)), nothing)
+    pass_on(1, 2)
+    pass_on(1, 3)
     landed(zkb.at[0, 0:3], 32)
     for o in (3, 5, 4):
-        for d in nearest:
+        for d in farthest:
             along_x(o, d).start()
     attend(
-        3 * BUNDLE, stage_first, False,
-        ((0, 2, 0), (1, 2, 1), (1, 2, 2), (2, 2, 3), (2, 3, 0), (3, 3, 1), (3, 3, 2)), nothing,
+        3 * BUNDLE, stage_first, 0,
+        ((1, 2, 1), (2, 2, 2), (3, 2, 3)), nothing,
     )
-    attend(2 * BUNDLE, stage_second, False, ((0, 3, 3),), nothing)
+    attend(2 * BUNDLE, stage_second, 0, (), nothing)
+    for j in range(NX):
+        landed(zka.at[0, 0:2], 25 + j)
     landed(zka.at[0], 29)
     landed(zkb.at[0:3], 33)
-    attend(LAST, stage_last, False, (), finish)
+    attend(LAST, stage_last, 0, (), finish)
 
     fetches[16].wait()
     fill = jnp.zeros((6, 128), F32)
@@ -534,6 +551,7 @@
     row_table, col_table = rope_constants()
     vmem = pltpu.VMEM
     dma = pltpu.SemaphoreType.DMA
+    hold = lambda a: pltpu.with_memory_space_constraint(a, pltpu.HBM)
     return pl.pallas_call(
         kernel,
         name="whole",
@@ -570,15 +588,15 @@
             dma((17,)), dma((3,)), dma((19,)), dma((42,)),
         ],
         compiler_params=pltpu.CompilerParams(
-            collective_id=0, has_side_effects=True, vmem_limit_bytes=60 * 1024 * 1024
+            collective_id=0, has_side_effects=True, vmem_limit_bytes=40 * 1024 * 1024
         ),
-    )(
+    )(*(hold(a) for a in (
         condition.reshape(1, -1), shift_weight, scale_weight, gate_weight,
         context_bias.reshape(1, -1), latent_in, norm_gain.reshape(1, -1),
         query_gain.reshape(1, -1), latent_gain.reshape(1, -1), jnp.asarray(row_table),
         jnp.asarray(col_table), context_latent, context_rope, down_query, down_latent,
         down_rope.T, up_query, up_key, up_value, out_weight,
-    )
+    )))
 
 
 def solution(mesh):

time: 61.3 us -> 58.7 us (0.958)
  Pallas kernels: 58.8 us -> 57.5 us
  local copies, waits for them, and re-layouts: 1.77 us -> 0.75 us
    pallas_call x1, Pallas kernels: 58.8 us -> 57.5 us  [on_device(): pl.pallas_call(kernel, name='whole', out_shape=jax.ShapeDtypeStruct((ROWS...]
    unnamed x1, local copies, waits for them, and re-layouts: 1.77 us -> 0.75 us
where the time goes in v5:
time: 58.7 us; the launch traced here: 58.2 us
  Pallas kernels  57.5 us (98%)
  local copies, waits for them, and re-layouts  0.75 us (1%)
    pallas_call x1, Pallas kernels, on_device(): pl.pallas_call(kernel, name='whole', out_shape=jax.ShapeDtypeStruct((ROWS...  57.5 us

profile of v5, /device:TPU:2, one launch (start us, length us, event | category | flops | bytes accessed | tf_op | source)
XLA Modules:
  0.0 58.2 jit_solution(74879084015189853)
XLA Ops:
  0.0 57.5 %whole.1 = bf16[96,2048]{1,0:T(8,128)(2,1)S(1)} custom-call(bf16[1,64]{1,0:T(2,128)(2,1)} %bitcast.10, bf16[64,512]{1,0:T(8,128)(2,1)} %sw_h.1, bf16[64,512]{1,0:T(8,128)(2,1)} %cw_h.1, bf16[64,512]{1,0:T(8,128)(2,1)} %gw_h.1, f32[1,2]{1,0:T(1,128)} %bitcast.11, bf16[96,2048]{1,0:T(8,128)(2,1)} %lat_h.1, f32[1,2048]{1,0:T(1,128)} %bitcast.7, ...), custom_call_target="tpu_custom_call" | custom-call | tf_op jit(solution)/shard_map/whole/pallas_call | solution.py:555
  57.5 0.7 %copy.22 = bf16[96,2048]{1,0:T(8,128)(2,1)} copy(bf16[96,2048]{1,0:T(8,128)(2,1)S(1)} %whole.1) | data formatting | bytes 786432

commit v6 on v5

--- a/solution.py
+++ b/solution.py
@@ -19,7 +19,7 @@
 ROWS_A, ROWS_B = 64, 32
 PIECE_A, PIECE_B = ROWS_A + 16, ROWS_B + 16
 BUNDLE = NX * ROWS_A
-LAST = 3 * BUNDLE + (NX - 1) * NZ * ROWS_B
+LAST = 3 * BUNDLE + (NX - 2) * NZ * ROWS_B
 LOG2E = math.log2(math.e)
 SCALE2 = LOG2E / math.sqrt(192.0)
 MESH = pl.DeviceIdType.MESH
@@ -285,7 +285,7 @@
 
     def along_x(o, d):
         held = zkb.at[x, slot_of(-o)]
-        return remote(held, held, snd.at[16], rcv.at[33], x=xp[d])
+        return remote(held, held, snd.at[16], rcv.at[42 if d == 1 else 33], x=xp[d])
 
     for d in farthest:
         kcopies[d - 1].start()
@@ -321,7 +321,27 @@
 
     landed(qa.at[0:3], 13)
 
+    def forward_second():
+        landed(zkb.at[0, 0:2], 30)
+        along_z(-2, 3, right).start()
+        along_z(2, 5, left).start()
+
+        @pl.when(z % 2 == 0)
+        def _():
+            along_z(-2, 4, zp[2]).start()
+
+        @pl.when(z % 2 == 1)
+        def _():
+            along_z(2, 4, zp[6]).start()
+
+        landed(zkb.at[0, 0:2], 31)
+        for o in (1, 7, 2, 6):
+            for d in range(1, NX):
+                along_x(o, d).start()
+
     for k in range(NY):
+        if k == 2:
+            forward_second()
         qt = dot_nt(wq_t[k], qa[...].reshape(QN, 512))
         for h in range(2):
             b = 192 * h
@@ -444,48 +464,35 @@
     def stage_second():
         stage_a(0, -2)
         stage_a(BUNDLE, 2)
+        stage_b(2 * BUNDLE, xp[NX - 1])
 
     def stage_last():
         for i, offset in enumerate((-3, 3, 4)):
             stage_a(i * BUNDLE, offset)
-        for d in range(1, NX):
-            stage_b((2 + d) * BUNDLE, xp[NX - d])
+        for d in range(2, NX):
+            stage_b((1 + d) * BUNDLE, xp[NX - d])
 
     def nothing(*_):
         pass
 
-    landed(zkb.at[0, 0:2], 30)
-    along_z(-2, 3, right).start()
-    along_z(2, 5, left).start()
-
-    @pl.when(z % 2 == 0)
-    def _():
-        along_z(-2, 4, zp[2]).start()
-
-    @pl.when(z % 2 == 1)
-    def _():
-        along_z(2, 4, zp[6]).start()
-
-    landed(zkb.at[0, 0:2], 31)
-    for o in (1, 7, 2, 6):
-        for d in farthest:
-            along_x(o, d).start()
-    attend(CTXK + BUNDLE, stage_own, CTXK, ((1, 2, 0), (3, 1, 1)), nothing)
+    attend(CTXK + BUNDLE, stage_own, CTXK, ((2, 2, 0), (3, 1, 1)), nothing)
     pass_on(1, 2)
     pass_on(1, 3)
     landed(zkb.at[0, 0:3], 32)
-    for o in (3, 5, 4):
-        for d in farthest:
+    for d in range(1, NX):
+        for o in (3, 5, 4):
             along_x(o, d).start()
     attend(
         3 * BUNDLE, stage_first, 0,
-        ((1, 2, 1), (2, 2, 2), (3, 2, 3)), nothing,
+        ((2, 2, 1), (3, 2, 2)), nothing,
     )
-    attend(2 * BUNDLE, stage_second, 0, (), nothing)
+    pass_on(2, 3)
+    landed(zkb.at[0], 42)
+    attend(3 * BUNDLE, stage_second, 0, (), nothing)
     for j in range(NX):
         landed(zka.at[0, 0:2], 25 + j)
     landed(zka.at[0], 29)
-    landed(zkb.at[0:3], 33)
+    landed(zkb.at[0:2], 33)
     attend(LAST, stage_last, 0, (), finish)
 
     fetches[16].wait()
@@ -585,7 +592,7 @@
             vmem((NY, 2, NY, ROWS, 128), BF16), vmem((NY, NY - 1, 2, ROWS, 128), BF16),
             vmem((NY, NY, 2, 128), F32), vmem((NY, NY - 1, 2, 128), F32),
             vmem((ROWS, D), F32),
-            dma((17,)), dma((3,)), dma((19,)), dma((42,)),
+            dma((17,)), dma((3,)), dma((19,)), dma((43,)),
         ],
         compiler_params=pltpu.CompilerParams(
             collective_id=0, has_side_effects=True, vmem_limit_bytes=40 * 1024 * 1024

time: 58.7 us -> 57.3 us (0.976)
  Pallas kernels: 57.5 us -> 56.5 us
    pallas_call x1, Pallas kernels: 57.5 us -> 56.5 us  [on_device(): pl.pallas_call(kernel, name='whole', out_shape=jax.ShapeDtypeStruct((ROWS...]
where the time goes in v6:
time: 57.3 us; the launch traced here: 57.2 us
  Pallas kernels  56.5 us (99%)
  local copies, waits for them, and re-layouts  0.75 us (1%)
    pallas_call x1, Pallas kernels, on_device(): pl.pallas_call(kernel, name='whole', out_shape=jax.ShapeDtypeStruct((ROWS...  56.5 us

profile of v6, /device:TPU:2, one launch (start us, length us, event | category | flops | bytes accessed | tf_op | source)
XLA Modules:
  0.0 57.2 jit_solution(14672444852661947606)
XLA Ops:
  0.0 56.5 %whole.1 = bf16[96,2048]{1,0:T(8,128)(2,1)S(1)} custom-call(bf16[1,64]{1,0:T(2,128)(2,1)} %bitcast.10, bf16[64,512]{1,0:T(8,128)(2,1)} %sw_h.1, bf16[64,512]{1,0:T(8,128)(2,1)} %cw_h.1, bf16[64,512]{1,0:T(8,128)(2,1)} %gw_h.1, f32[1,2]{1,0:T(1,128)} %bitcast.11, bf16[96,2048]{1,0:T(8,128)(2,1)} %lat_h.1, f32[1,2048]{1,0:T(1,128)} %bitcast.7, ...), custom_call_target="tpu_custom_call" | custom-call | tf_op jit(solution)/shard_map/whole/pallas_call | solution.py:562
  56.5 0.7 %copy.22 = bf16[96,2048]{1,0:T(8,128)(2,1)} copy(bf16[96,2048]{1,0:T(8,128)(2,1)S(1)} %whole.1) | data formatting | bytes 786432

commit v7 on v6

--- a/solution.py
+++ b/solution.py
@@ -323,8 +323,6 @@
 
     def forward_second():
         landed(zkb.at[0, 0:2], 30)
-        along_z(-2, 3, right).start()
-        along_z(2, 5, left).start()
 
         @pl.when(z % 2 == 0)
         def _():
@@ -333,6 +331,9 @@
         @pl.when(z % 2 == 1)
         def _():
             along_z(2, 4, zp[6]).start()
+
+        along_z(-2, 3, right).start()
+        along_z(2, 5, left).start()
 
         landed(zkb.at[0, 0:2], 31)
         for o in (1, 7, 2, 6):
@@ -340,7 +341,7 @@
                 along_x(o, d).start()
 
     for k in range(NY):
-        if k == 2:
+        if k == 1:
             forward_second()
         qt = dot_nt(wq_t[k], qa[...].reshape(QN, 512))
         for h in range(2):

time: 57.3 us -> 57.2 us (level)
  no operation moved by 1% of the time
where the time goes in v7:
time: 57.2 us; the launch traced here: 57 us
  Pallas kernels  56.2 us (98%)
  local copies, waits for them, and re-layouts  0.75 us (1%)
    pallas_call x1, Pallas kernels, on_device(): pl.pallas_call(kernel, name='whole', out_shape=jax.ShapeDtypeStruct((ROWS...  56.2 us

profile of v7, /device:TPU:2, one launch (start us, length us, event | category | flops | bytes accessed | tf_op | source)
XLA Modules:
  0.0 57.0 jit_solution(4881672450155320692)
XLA Ops:
  0.0 56.2 %whole.1 = bf16[96,2048]{1,0:T(8,128)(2,1)S(1)} custom-call(bf16[1,64]{1,0:T(2,128)(2,1)} %bitcast.10, bf16[64,512]{1,0:T(8,128)(2,1)} %sw_h.1, bf16[64,512]{1,0:T(8,128)(2,1)} %cw_h.1, bf16[64,512]{1,0:T(8,128)(2,1)} %gw_h.1, f32[1,2]{1,0:T(1,128)} %bitcast.11, bf16[96,2048]{1,0:T(8,128)(2,1)} %lat_h.1, f32[1,2048]{1,0:T(1,128)} %bitcast.7, ...), custom_call_target="tpu_custom_call" | custom-call | tf_op jit(solution)/shard_map/whole/pallas_call | solution.py:563
  56.2 0.7 %copy.22 = bf16[96,2048]{1,0:T(8,128)(2,1)} copy(bf16[96,2048]{1,0:T(8,128)(2,1)S(1)} %whole.1) | data formatting | bytes 786432
